TPU v7x, 256 devices: a whole 4x4x8 slice. The times are simulated.
256 devices in a mesh: sp: 64 (over z, y, core), tp: 4 (over x).
Axes of the slice: x: 4, y: 4, z: 8, core: 2. Of those that a mesh axis runs over, the one named last changes fastest.
Arguments:
- stream: bfloat16 [32768, 2048], P('sp', 'tp'), may hold values from -6 to 6
- doc_ids: int32 [32768], P('sp'), may hold values from 0 to 15, never falling along the last dimension, each value on 1 to 16640 neighbouring positions
- norm_gain: float32 [2, 2048], replicated, may hold values from 0.1 to 1.9
- gate_proj: bfloat16 [2, 2048, 2048], P(None, 'sp', 'tp'), may hold values from -0.125 to 0.125
- input_gate: bfloat16 [2, 2048, 2048], P(None, 'sp', 'tp'), may hold values from -0.125 to 0.125
- value_proj: bfloat16 [2, 2048, 2048], P(None, 'sp', 'tp'), may hold values from -0.125 to 0.125
- taps: float32 [2, 3, 2048], P(None, None, 'tp'), may hold values from -3 to 3
- out_proj: bfloat16 [2, 2048, 2048], P(None, 'tp', 'sp'), may hold values from -0.125 to 0.125
Outputs:
- result: bfloat16 [32768, 2048], P('sp', 'tp')
Inputs may be any that keep to these rules, and one draw needn't show every extreme that they name: `doc_ids`: document numbers never fall along the sequence; each document holds 1 to 16640 positions.
All inputs are finite; a program needn't handle non-finite values.
Results may differ from a plain program's by a relative error of at most 0.03.
Values may be sent and summed in bfloat16 or wider, within the bound.
No kernel may reach another device: no remote copies, remote signals or barrier semaphores. Data moves between devices by JAX's collectives and lax.ppermute only.
A program may use at most 64 MiB of HBM per device.

v0:
```python
import functools

import jax
import jax.numpy as jnp
from jax import lax
from jax.experimental import pallas as pl
from jax.experimental.pallas import tpu as pltpu
from jax.sharding import Mesh
from jax.sharding import PartitionSpec as P


epsilon = 1e-06
NZ, NY, NC, NX = 8, 4, 2, 4
SP = ("z", "y", "c")
HALO = 8
VMEM_LIMIT = 26


def partner(value):
    return lax.ppermute(value, "c", [(0, 1), (1, 0)])


def onward(value, axis, step=1):
    size = lax.axis_size(axis)
    pairs = [(2 * i, 2 * ((i + step) % size)) for i in range(size)]
    pairs += [(2 * i + 1, 2 * ((i - step) % size) + 1) for i in range(size)]
    return lax.ppermute(value, (axis, "c"), pairs)


def shifted(value, axis, step):
    size = lax.axis_size(axis)
    return lax.ppermute(value, axis, [(i, (i + step) % size) for i in range(size)])


def with_edges(value, c):
    size = lax.axis_size(SP)
    first, last = value[:HALO], value[-HALO:]
    both = lax.all_gather(jnp.concatenate([first, last], axis=0), "c", axis=0)
    pairs = [(i, i - 1) for i in range(2, size, 2)] + [(i, i + 1) for i in range(1, size - 1, 2)]
    outer = lax.ppermute(jnp.where(c == 0, first, last), SP, pairs)
    before = jnp.where(c == 0, outer, both[0, HALO:])
    after = jnp.where(c == 0, both[1, :HALO], outer)
    return jnp.concatenate([before, value, after], axis=0)


def half(units, c):
    count = units.shape[0] // 2
    return lax.dynamic_slice_in_dim(units, c * count, count, axis=0)


def by_y_then_z(own, c):
    near = onward(own, "y")
    opposite = onward(half(own, c), "y", 2)
    mixed = jnp.concatenate([half(own, c), near, opposite], axis=0)
    if own.shape[0] == 2:
        around = lax.all_gather(mixed, "c", axis=0, tiled=True)
    else:
        other = partner(mixed)
        around = jnp.where(c == 0, jnp.concatenate([mixed, other]), jnp.concatenate([other, mixed]))
    moved = [around]
    for _ in range(3):
        moved.append(onward(moved[-1], "z"))
    moved = moved[1:] + [onward(half(moved[-1], c), "z")]
    return [around] + moved + [partner(jnp.concatenate(moved[k : k + 2], axis=0)) for k in (0, 2)]


def by_z_then_y(own, c):
    one = onward(own, "z")
    two = onward(own, "z", 2)
    far = onward(jnp.concatenate([one, half(two, c)], axis=0), "z", 2)
    side = jnp.concatenate([half(own, c), one, two, far], axis=0)
    side = lax.optimization_barrier(side)
    around = jnp.concatenate([partner(side), side], axis=0)
    near = onward(around, "y")
    moved = [near, onward(near[near.shape[0] // 2 :], "y")]
    return [around] + moved + [partner(jnp.concatenate(moved, axis=0))]


def units_of(layer_index, y, z, c, s):
    def a(units, off):
        return [(m, lax.rem(z + off + NZ, NZ), lax.rem(y + y_off + NY, NY)) for m, y_off in units]

    def b(units, off):
        return [(m, lax.rem(z + z_off + NZ, NZ), lax.rem(y + off + NY, NY)) for m, z_off in units]

    count = 1 if layer_index == 0 else 2

    def mixed(c, s):
        halves = [count * c + k for k in range(count)]
        near = [(m, s) for m in range(2 * count)]
        return [(m, 0) for m in halves] + near + [(m, 2) for m in halves]

    both = mixed(0, -1) + mixed(1, 1)

    def moved_a(c, s):
        return [a(both, k * s) for k in (1, 2, 3)] + [a(mixed(c, s), 4)]

    theirs = moved_a(1 - c, -s)
    first = [a(both, 0)] + moved_a(c, s) + [theirs[0] + theirs[1], theirs[2] + theirs[3]]
    if layer_index == 1:
        return first

    def side(c, s):
        return [(2 + c, 0)] + [(m, k * s) for k in (1, 2, 3) for m in (2, 3)] + [(2 + c, 4)]

    def around_b(c, s):
        return side(1 - c, -s) + side(c, s)

    def moved_b(c, s):
        return [b(around_b(c, s), s), b(side(c, s), 2)]

    theirs = moved_b(1 - c, -s)
    return first + [b(around_b(c, s), 0)] + moved_b(c, s) + [theirs[0] + theirs[1]]


def gather_first(rows):
    copies = jnp.broadcast_to(rows, (lax.axis_size("x"), *rows.shape))
    return lax.all_to_all(copies, "x", 0, 0, tiled=True)


def gather_x(rows, cut):
    left = shifted(rows, "x", 1)
    right = shifted(rows, "x", -1)
    return [rows, left, right, shifted(left[:cut], "x", 1), shifted(right[cut:], "x", -1)]


def wide(value):
    return value.astype(jnp.float32)


def joined(near, far):
    return (wide(near) + wide(far)).astype(jnp.bfloat16)


def scatter_x(rows, own, right, left, far_top, far_bottom):
    cut = far_top.shape[0]
    got_top = shifted(far_top, "x", 1)
    got_bottom = shifted(far_bottom, "x", -1)
    right = jnp.concatenate([joined(right[:cut], got_top), right[cut:]], axis=0)
    left = jnp.concatenate([left[:cut], joined(left[cut:], got_bottom)], axis=0)
    from_left = shifted(right, "x", 1)
    from_right = shifted(left, "x", -1)
    return (wide(rows) + (wide(own) + wide(from_left) + wide(from_right))).astype(jnp.bfloat16)


def layer_kernel(index, cut, n_sources, n_pieces, *refs):
    sources, refs = refs[:n_sources], refs[n_sources:]
    (gains, same_ref, taps), refs = refs[:3], refs[3:]
    pieces, refs = refs[:n_pieces], refs[n_pieces:]
    outs, (normed, gated, weights) = refs[:5], refs[5:]
    x, y, z, c = (lax.axis_index(name) for name in ("x", "y", "z", "c"))
    blocks = [lax.rem(x + off + NX, NX) for off in (0, -1, 1, 2)] if n_sources > 1 else list(range(NX))

    step = 16
    for base, count in ((0, cut), (cut, normed.shape[0] - cut)):

        def normalise(i, carry, base=base):
            here = pl.ds(pl.multiple_of(i * step, step), step)
            there = pl.ds(pl.multiple_of(base + i * step, step), step)
            if n_sources > 1:
                values = [source[there, :].astype(jnp.float32) for source in sources[:3]]
                values.append(sources[3 if base == 0 else 4][here, :].astype(jnp.float32))
            else:
                values = [sources[0][block, there, :].astype(jnp.float32) for block in blocks]
            total = sum(jnp.sum(v * v, axis=1, keepdims=True) for v in values)
            scale = lax.rsqrt(total * (1.0 / (512 * NX)) + epsilon)
            for block, v in zip(blocks, values):
                columns = pl.ds(pl.multiple_of(block * 512, 512), 512)
                scaled = v * scale * gains[index, pl.ds(block, 1), :]
                normed[there, columns] = scaled.astype(jnp.bfloat16)
            return carry

        steps = count // step
        lax.fori_loop(0, steps, normalise, 0, unroll=2 if steps % 2 == 0 else 1)

    for piece, units in zip(pieces, units_of(index, y, z, c, 2 * c - 1)):
        for k, (mat, z_at, y_at) in enumerate(units):
            row = pl.multiple_of(z_at * 256 + y_at * 64, 64)
            weights[mat, pl.ds(row, 64), :] = piece[k]

    rows = normed.shape[0]
    same = same_ref[...]
    same_before, same_after = same[:, 0:1] > 0.5, same[:, 1:2] > 0.5

    def mix(n, carry):
        columns = pl.ds(pl.multiple_of(n * 256, 256), 256)

        def project(mat):
            value = jnp.dot(normed[...], weights[mat, :, columns], preferred_element_type=jnp.float32)
            return value.astype(jnp.bfloat16).astype(jnp.float32)

        mixed = (project(0) * project(1)).astype(jnp.bfloat16).astype(jnp.float32)
        before = pltpu.roll(mixed, 1, 0)
        after = pltpu.roll(mixed, rows - 1, 0)
        convolved = (
            jnp.where(same_before, taps[index, 0:1, columns] * before, 0.0)
            + taps[index, 1:2, columns] * mixed
            + jnp.where(same_after, taps[index, 2:3, columns] * after, 0.0)
        )
        gated[:, columns] = (project(2) * convolved).astype(jnp.bfloat16)
        return carry

    lax.fori_loop(0, 2, mix, 0)

    for place, off in enumerate((0, 1, -1, 2)):
        block = lax.rem(x + off + NX, NX)

        def project_out(n, carry, place=place, block=block):
            value = lax.dot_general(
                gated[...],
                weights[3, pl.ds(pl.multiple_of(block * 512 + n * 256, 256), 256), :],
                (((1,), (1,)), ((), ())),
                preferred_element_type=jnp.float32,
            ).astype(jnp.bfloat16)
            columns = pl.ds(pl.multiple_of(n * 256, 256), 256)
            if place < 3:
                outs[place][:, columns] = value
            else:
                outs[3][:, columns] = value[:cut]
                outs[4][:, columns] = value[cut:]
            return carry

        lax.fori_loop(0, 2, project_out, 0)


def layer(index, cut, sources, gains, same, taps, pieces):
    rows = same.shape[0]
    vmem = pl.BlockSpec(memory_space=pltpu.VMEM)
    return pl.pallas_call(
        functools.partial(layer_kernel, index, cut, len(sources), len(pieces)),
        out_shape=[jax.ShapeDtypeStruct((n, 512), jnp.bfloat16) for n in (rows, rows, rows, cut, rows - cut)],
        in_specs=[vmem] * (len(sources) + 3 + len(pieces)),
        out_specs=[vmem] * 5,
        scratch_shapes=[
            pltpu.VMEM((rows, 2048), jnp.bfloat16),
            pltpu.VMEM((rows, 512), jnp.bfloat16),
            pltpu.VMEM((4, 2048, 512), jnp.bfloat16),
        ],
        compiler_params=pltpu.CompilerParams(vmem_limit_bytes=VMEM_LIMIT << 20),
        cost_estimate=pl.CostEstimate(flops=2 * rows * 2048 * 2048, bytes_accessed=8 << 20, transcendentals=rows),
    )(*sources, gains, same, taps, *pieces)


def per_device(stream, doc_ids, norm_gain, gate_proj, input_gate, value_proj, taps, out_proj):
    c = lax.axis_index("c")
    mats = jnp.stack([input_gate, value_proj, gate_proj, jnp.swapaxes(out_proj, 1, 2)], axis=1)
    chip = lax.all_gather(mats, "c", axis=2, tiled=True)

    ids = jnp.broadcast_to(doc_ids.astype(jnp.bfloat16)[:, None], (doc_ids.shape[0], 128))
    wider = with_edges(jnp.concatenate([stream, ids], axis=1), c)
    rows = wider[:, :512]
    gathered = gather_first(rows)
    me, length = lax.axis_index(SP), doc_ids.shape[0]
    docs = wider[:, 512].astype(jnp.float32)
    place = lax.broadcasted_iota(jnp.int32, (length + 2 * HALO,), 0) + me * length
    docs = jnp.where((place < HALO) | (place >= lax.axis_size(SP) * length + HALO), -1.0, docs)
    equal = (docs[1:] == docs[:-1]).astype(jnp.float32)
    none = jnp.zeros((1,), jnp.float32)
    same = jnp.stack([jnp.concatenate([none, equal]), jnp.concatenate([equal, none])], axis=1)
    gains = norm_gain.reshape(-1, NX, 512)
    pieces = [by_y_then_z(chip[0, :2], c) + by_z_then_y(chip[0, 2:], c), by_y_then_z(chip[1], c)]

    cut = (rows.shape[0] // 32 + 1) * 16
    sources = [gathered]
    for index in range(2):
        parts = layer(index, cut, sources, gains, same, taps, pieces[index])
        rows = scatter_x(rows, *parts)
        if index == 0:
            sources = gather_x(rows, cut)
    return rows[HALO:-HALO]


def solution(mesh):
    split = Mesh(mesh.devices.reshape(NZ, NY, NC, NX), ("z", "y", "c", "x"))
    in_specs = (
        P(SP, "x"),
        P(SP),
        P(),
        P(None, SP, "x"),
        P(None, SP, "x"),
        P(None, SP, "x"),
        P(None, None, "x"),
        P(None, "x", SP),
    )

    return jax.shard_map(per_device, mesh=split, in_specs=in_specs, out_specs=P(SP, "x"), check_vma=False)
```

profile of v0, /device:TPU:1, one launch (start us, length us, event | category | flops | bytes accessed | tf_op | source)
XLA Modules:
  0.0 220.1 jit_solution(1031594165106171791)
XLA Ops:
  0.0 1.0 pad_maximum_fusion.13
  1.0 5.0 %all_gather.14 = bf16[2,4,64,512]{3,2,1,0:T(8,128)(2,1)S(1)} all-gather(bf16[2,4,32,512]{3,2,1,0:T(8,128)(2,1)S(1)} %pad_maximum_fusion.13), channel_id=1, replica_groups=mesh['z'=8,'y'=4,'c'=2,'x'=4] {'c'}, dimensions={2}, use_global_device_ids=true | all-gather | bytes 786432 | tf_op jit(solution)/shard_map/all_gather | solution.py:247
  6.7 4.3 %collective-permute-start.10 = (bf16[2,64,512]{2,1,0:T(8,128)(2,1)S(1)}, bf16[2,64,512]{2,1,0:T(8,128)(2,1)S(1)}, u32[]{:S(2)}, u32[]{:S(2)}) collective-permute-start(bf16[2,64,512]{2,1,0:T(8,128)(2,1)S(1)} %get-tuple-element.32), channel_id=1, source_target_pairs={{0,64},{32,96},{64,128},{96,160},{128,192},{160,224},{192,0},{224,... | collective-permute-start | bytes 393224 | tf_op jit(solution)/shard_map/ppermute | solution.py:27
  11.7 2.6 %collective-permute-done.10 = bf16[2,64,512]{2,1,0:T(8,128)(2,1)S(1)} collective-permute-done((bf16[2,64,512]{2,1,0:T(8,128)(2,1)S(1)}, bf16[2,64,512]{2,1,0:T(8,128)(2,1)S(1)}, u32[]{:S(2)}, u32[]{:S(2)}) %collective-permute-start.10) | collective-permute-done | bytes 131104 | tf_op jit(solution)/shard_map/ppermute | solution.py:27
  14.3 1.6 collective-permute-done.9
  16.0 2.5 %collective-permute-start.11 = (bf16[3,64,512]{2,1,0:T(8,128)(2,1)S(1)}, bf16[3,64,512]{2,1,0:T(8,128)(2,1)S(1)}, u32[]{:S(2)}, u32[]{:S(2)}) collective-permute-start(bf16[3,64,512]{2,1,0:T(8,128)(2,1)S(1)} %pad_maximum_fusion.15), channel_id=1, source_target_pairs={{0,64},{32,96},{64,128},{96,160},{128,192},{160,224},{192,0},{224,... | collective-permute-start | bytes 589832 | tf_op jit(solution)/shard_map/ppermute | solution.py:27
  18.5 4.3 %collective-permute-done.11 = bf16[3,64,512]{2,1,0:T(8,128)(2,1)S(1)} collective-permute-done((bf16[3,64,512]{2,1,0:T(8,128)(2,1)S(1)}, bf16[3,64,512]{2,1,0:T(8,128)(2,1)S(1)}, u32[]{:S(2)}, u32[]{:S(2)}) %collective-permute-start.11) | collective-permute-done | bytes 196640 | tf_op jit(solution)/shard_map/ppermute | solution.py:27
  22.9 4.0 %collective-permute-start.12 = (bf16[8,64,512]{2,1,0:T(8,128)(2,1)S(1)}, bf16[8,64,512]{2,1,0:T(8,128)(2,1)}, u32[]{:S(2)}, u32[]{:S(2)}) collective-permute-start(bf16[8,64,512]{2,1,0:T(8,128)(2,1)S(1)} %pad_maximum_fusion.11), channel_id=1, source_target_pairs={{0,4},{4,0},{1,5},{5,1},{2,6},{6,2},{3,7},{7,3},{8,12},{12,8},{9,1... | collective-permute-start | bytes 1572872 | tf_op jit(solution)/shard_map/ppermute | solution.py:20
  26.9 2.8 %collective-permute-start.24 = (bf16[4,64,512]{2,1,0:T(8,128)(2,1)S(1)}, bf16[4,64,512]{2,1,0:T(8,128)(2,1)S(1)}, u32[]{:S(2)}, u32[]{:S(2)}) collective-permute-start(bf16[4,64,512]{2,1,0:T(8,128)(2,1)S(1)} %get-tuple-element.28), channel_id=1, source_target_pairs={{0,8},{8,16},{16,24},{24,0},{4,28},{12,4},{20,12},{28,20},{1,9},{9... | collective-permute-start | bytes 786440 | tf_op jit(solution)/shard_map/ppermute | solution.py:27
  30.2 0.8 collective-permute-start.1
  30.9 5.9 %collective-permute-done.25 = bf16[2,64,512]{2,1,0:T(8,128)(2,1)S(1)} collective-permute-done((bf16[2,64,512]{2,1,0:T(8,128)(2,1)S(1)}, bf16[2,64,512]{2,1,0:T(8,128)(2,1)S(1)}, u32[]{:S(2)}, u32[]{:S(2)}) %collective-permute-start.25) | collective-permute-done | bytes 131104 | tf_op jit(solution)/shard_map/ppermute | solution.py:27
  36.9 2.0 collective-permute-start.26
  38.9 1.1 pad_maximum_fusion.4.refs_11_
  40.4 0.8 collective-permute-start.2
  41.1 4.6 %collective-permute-done.2 = bf16[1,64,512]{2,1,0:T(8,128)(2,1)S(1)} collective-permute-done((bf16[1,64,512]{2,1,0:T(8,128)(2,1)S(1)}, bf16[1,64,512]{2,1,0:T(8,128)(2,1)S(1)}, u32[]{:S(2)}, u32[]{:S(2)}) %collective-permute-start.2) | collective-permute-done | bytes 65568 | tf_op jit(solution)/shard_map/ppermute | solution.py:27
  45.7 0.9 pad_maximum_fusion.14
  46.7 13.0 %all_gather.15.refs_4_ = bf16[8,64,512]{2,1,0:T(8,128)(2,1)S(1)} all-gather(bf16[4,64,512]{2,1,0:T(8,128)(2,1)S(1)} %pad_maximum_fusion.14), channel_id=1, replica_groups=mesh['z'=8,'y'=4,'c'=2,'x'=4] {'c'}, dimensions={0}, use_global_device_ids=true | all-gather | bytes 786432 | tf_op jit(solution)/shard_map/all_gather | solution.py:56
  60.0 1.5 maximum_select_fusion.refs_8_
  61.5 1.7 collective-permute-start.27
  63.2 4.8 %collective-permute-done.3.refs_5_ = bf16[8,64,512]{2,1,0:T(8,128)(2,1)S(1)} collective-permute-done((bf16[8,64,512]{2,1,0:T(8,128)(2,1)S(1)}, bf16[8,64,512]{2,1,0:T(8,128)(2,1)S(1)}, u32[]{:S(2)}, u32[]{:S(2)}) %collective-permute-start.3) | collective-permute-done | bytes 524320 | tf_op jit(solution)/shard_map/ppermute | solution.py:27
  68.0 1.2 collective-permute-start.4
  69.2 0.9 slice.97
  70.1 1.5 collective-permute-start.14
  71.8 2.2 %collective-permute-start = (bf16[8,640]{1,0:T(8,128)(2,1)S(1)}, bf16[8,640]{1,0:T(8,128)(2,1)S(1)}, u32[]{:S(2)}, u32[]{:S(2)}) collective-permute-start(bf16[8,640]{1,0:T(8,128)(2,1)S(1)} %get-tuple-element.25), channel_id=1, source_target_pairs={{8,4},{16,12},{24,20},{32,28},{40,36},{48,44},{56,52},{64,60},{72,... | collective-permute-start | bytes 30728 | tf_op jit(solution)/shard_map/ppermute | solution.py:40
  74.0 1.8 all-gather
  75.9 1.4 collective-permute-done
  77.3 7.7 %collective-permute-done.4.refs_6_ = bf16[8,64,512]{2,1,0:T(8,128)(2,1)} collective-permute-done((bf16[8,64,512]{2,1,0:T(8,128)(2,1)S(1)}, bf16[8,64,512]{2,1,0:T(8,128)(2,1)}, u32[]{:S(2)}, u32[]{:S(2)}) %collective-permute-start.4) | collective-permute-done | bytes 524320 | tf_op jit(solution)/shard_map/ppermute | solution.py:27
  85.0 1.1 collective-permute-start.5
  86.2 0.9 copy-done.13
  87.1 1.5 broadcast_in_dim.14
  88.7 4.5 %all-to-all-start = ((bf16[4,528,512]{2,1,0:T(8,128)(2,1)}), bf16[4,528,512]{2,1,0:T(8,128)(2,1)}, u32[]{:S(2)}, u32[]{:S(2)}) async-start(bf16[4,528,512]{2,1,0:T(8,128)(2,1)} %broadcast_in_dim.14), calls=%async_computation | async-start | bytes 4325376 | tf_op jit(solution)/shard_map/all_to_all | solution.py:118
  93.2 1.0 collective-permute-start.28
  94.2 2.3 %pad_maximum_fusion.1 = bf16[24,64,512]{2,1,0:T(8,128)(2,1)} fusion(bf16[8,64,512]{2,1,0:T(8,128)(2,1)} %collective-permute-done.14.refs_13_, bf16[16,64,512]{2,1,0:T(8,128)(2,1)S(1)} %collective-permute-done.13.refs_12_), kind=kLoop, calls=%fused_computation.1 | loop fusion | flops 786432 | bytes 3145728 | tf_op jit(solution)/shard_map/concatenate | solution.py:76
  97.0 3.0 %collective-permute-start.6 = (bf16[4,64,512]{2,1,0:T(8,128)(2,1)S(1)}, bf16[4,64,512]{2,1,0:T(8,128)(2,1)S(1)}, u32[]{:S(2)}, u32[]{:S(2)}) collective-permute-start(bf16[4,64,512]{2,1,0:T(8,128)(2,1)S(1)} %constant_dynamic-slice_fusion.2), channel_id=1, source_target_pairs={{0,32},{32,64},{64,96},{96,128},{128,160},{160,192},{192,224},{224... | collective-permute-start | bytes 786440 | tf_op jit(solution)/shard_map/ppermute | solution.py:27
  100.0 2.1 pad_maximum_fusion.3
  102.1 8.2 %collective-permute-done.6.refs_8_ = bf16[4,64,512]{2,1,0:T(8,128)(2,1)S(1)} collective-permute-done((bf16[4,64,512]{2,1,0:T(8,128)(2,1)S(1)}, bf16[4,64,512]{2,1,0:T(8,128)(2,1)S(1)}, u32[]{:S(2)}, u32[]{:S(2)}) %collective-permute-start.6) | collective-permute-done | bytes 262176 | tf_op jit(solution)/shard_map/ppermute | solution.py:27
  110.3 1.0 pad_maximum_fusion.5
  111.3 3.2 %collective-permute-start.8 = (bf16[12,64,512]{2,1,0:T(8,128)(2,1)}, bf16[12,64,512]{2,1,0:T(8,128)(2,1)}, u32[]{:S(2)}, u32[]{:S(2)}) collective-permute-start(bf16[12,64,512]{2,1,0:T(8,128)(2,1)} %pad_maximum_fusion.5), channel_id=1, source_target_pairs={{0,4},{4,0},{1,5},{5,1},{2,6},{6,2},{3,7},{7,3},{8,12},{12,8},{9,1... | collective-permute-start | bytes 2359304 | tf_op jit(solution)/shard_map/ppermute | solution.py:20
  114.7 1.8 collective-permute-start.29
  116.9 2.2 %all-to-all-done.refs_0_ = bf16[4,528,512]{2,1,0:T(8,128)(2,1)} async-done(((bf16[4,528,512]{2,1,0:T(8,128)(2,1)}), bf16[4,528,512]{2,1,0:T(8,128)(2,1)}, u32[]{:S(2)}, u32[]{:S(2)}) %all-to-all-start) | async-done | bytes 2162720 | tf_op jit(solution)/shard_map/all_to_all | solution.py:118
  119.2 1.2 copy-done.3
  120.4 1.0 copy-done.8
  121.4 0.9 copy-done.10
  122.4 13.4 %shard_map.82 = (bf16[528,512]{1,0:T(8,128)(2,1)S(1)}, bf16[528,512]{1,0:T(8,128)(2,1)S(1)}, bf16[528,512]{1,0:T(8,128)(2,1)S(1)}, bf16[272,512]{1,0:T(8,128)(2,1)S(1)}, bf16[256,512]{1,0:T(8,128)(2,1)S(1)}) custom-call(bf16[4,528,512]{2,1,0:T(8,128)(2,1)} %all-to-all-done.refs_0_, f32[2,4,512]{2,1,0:T(4,128)S(1)} %reshape.9.refs_1_.refs_5_, ...), custom_call_target="tpu_custom_call" | custom-call | flops 4429185024 | bytes 8388608 | tf_op jit(solution)/shard_map/pallas_call | solution.py:229
  135.7 1.0 collective-permute-start.18
  136.7 1.7 pad_maximum_fusion
  138.4 2.5 %collective-permute-start.31 = (bf16[32,64,512]{2,1,0:T(8,128)(2,1)S(1)}, bf16[32,64,512]{2,1,0:T(8,128)(2,1)S(1)}, u32[]{:S(2)}, u32[]{:S(2)}) collective-permute-start(bf16[32,64,512]{2,1,0:T(8,128)(2,1)S(1)} %pad_maximum_fusion), channel_id=1, source_target_pairs={{0,4},{4,0},{1,5},{5,1},{2,6},{6,2},{3,7},{7,3},{8,12},{12,8},{9,1... | collective-permute-start | bytes 6291464 | tf_op jit(solution)/shard_map/ppermute | solution.py:20
  141.0 1.0 collective-permute-start.30
  142.7 2.4 %collective-permute-start.19 = (bf16[528,512]{1,0:T(8,128)(2,1)S(1)}, bf16[528,512]{1,0:T(8,128)(2,1)S(1)}, u32[]{:S(2)}, u32[]{:S(2)}) collective-permute-start(bf16[528,512]{1,0:T(8,128)(2,1)S(1)} %pad_maximum_fusion.8), channel_id=1, source_target_pairs={{0,3},{1,0},{2,1},{3,2},{4,7},{5,4},{6,5},{7,6},{8,11},{9,8},{10,9... | collective-permute-start | bytes 1622024 | tf_op jit(solution)/shard_map/ppermute | solution.py:32
  145.1 6.5 %collective-permute-done.16 = bf16[272,512]{1,0:T(8,128)(2,1)S(1)} collective-permute-done((bf16[272,512]{1,0:T(8,128)(2,1)S(1)}, bf16[272,512]{1,0:T(8,128)(2,1)S(1)}, u32[]{:S(2)}, u32[]{:S(2)}) %collective-permute-start.16) | collective-permute-done | bytes 278560 | tf_op jit(solution)/shard_map/ppermute | solution.py:32
  152.8 2.1 collective-permute-done.19
  154.9 11.3 %collective-permute-done.17 = bf16[528,512]{1,0:T(8,128)(2,1)S(1)} collective-permute-done((bf16[528,512]{1,0:T(8,128)(2,1)S(1)}, bf16[528,512]{1,0:T(8,128)(2,1)S(1)}, u32[]{:S(2)}, u32[]{:S(2)}) %collective-permute-start.17) | collective-permute-done | bytes 540704 | tf_op jit(solution)/shard_map/ppermute | solution.py:32
  166.7 2.7 %collective-permute-start.21 = (bf16[528,512]{1,0:T(8,128)(2,1)S(1)}, bf16[528,512]{1,0:T(8,128)(2,1)S(1)}, u32[]{:S(2)}, u32[]{:S(2)}) collective-permute-start(bf16[528,512]{1,0:T(8,128)(2,1)S(1)} %add_convert_fusion.refs_0_), channel_id=1, source_target_pairs={{0,3},{1,0},{2,1},{3,2},{4,7},{5,4},{6,5},{7,6},{8,11},{9,8},{10,9... | collective-permute-start | bytes 1622024 | tf_op jit(solution)/shard_map/ppermute | solution.py:32
  169.3 10.9 %collective-permute-done.20.refs_1_ = bf16[528,512]{1,0:T(8,128)(2,1)S(1)} collective-permute-done((bf16[528,512]{1,0:T(8,128)(2,1)S(1)}, bf16[528,512]{1,0:T(8,128)(2,1)S(1)}, u32[]{:S(2)}, u32[]{:S(2)}) %collective-permute-start.20) | collective-permute-done | bytes 540704 | tf_op jit(solution)/shard_map/ppermute | solution.py:32
  180.3 2.7 %collective-permute-start.23 = (bf16[256,512]{1,0:T(8,128)(2,1)S(1)}, bf16[256,512]{1,0:T(8,128)(2,1)S(1)}, u32[]{:S(2)}, u32[]{:S(2)}) collective-permute-start(bf16[256,512]{1,0:T(8,128)(2,1)S(1)} %slice.99), channel_id=1, source_target_pairs={{0,3},{1,0},{2,1},{3,2},{4,7},{5,4},{6,5},{7,6},{8,11},{9,8},{10,9... | collective-permute-start | bytes 786440 | tf_op jit(solution)/shard_map/ppermute | solution.py:32
  183.1 3.3 %collective-permute-done.23.refs_4_ = bf16[256,512]{1,0:T(8,128)(2,1)S(1)} collective-permute-done((bf16[256,512]{1,0:T(8,128)(2,1)S(1)}, bf16[256,512]{1,0:T(8,128)(2,1)S(1)}, u32[]{:S(2)}, u32[]{:S(2)}) %collective-permute-start.23) | collective-permute-done | bytes 262176 | tf_op jit(solution)/shard_map/ppermute | solution.py:32
  186.4 1.0 collective-permute-done.22.refs_3_
  187.4 11.9 %shard_map.83 = (bf16[528,512]{1,0:T(8,128)(2,1)S(1)}, bf16[528,512]{1,0:T(8,128)(2,1)S(1)}, bf16[528,512]{1,0:T(8,128)(2,1)S(1)}, bf16[272,512]{1,0:T(8,128)(2,1)S(1)}, bf16[256,512]{1,0:T(8,128)(2,1)S(1)}) custom-call(bf16[528,512]{1,0:T(8,128)(2,1)S(1)} %add_convert_fusion.refs_0_, bf16[528,512]{1,0:T(8,128)(2,1)S(1)} %collective-permute-done.20.refs_1_, ...), custom_call_target="tpu_custom_call" | custom-call | flops 4429185024 | bytes 8388608 | tf_op jit(solution)/shard_map/pallas_call | solution.py:229
  199.3 2.2 %collective-permute-start.35 = (bf16[256,512]{1,0:T(8,128)(2,1)S(1)}, bf16[256,512]{1,0:T(8,128)(2,1)S(1)}, u32[]{:S(2)}, u32[]{:S(2)}) collective-permute-start(bf16[256,512]{1,0:T(8,128)(2,1)S(1)} %get-tuple-element.24), channel_id=1, source_target_pairs={{0,3},{1,0},{2,1},{3,2},{4,7},{5,4},{6,5},{7,6},{8,11},{9,8},{10,9... | collective-permute-start | bytes 786440 | tf_op jit(solution)/shard_map/ppermute | solution.py:32
  201.7 3.2 %collective-permute-done.35 = bf16[256,512]{1,0:T(8,128)(2,1)S(1)} collective-permute-done((bf16[256,512]{1,0:T(8,128)(2,1)S(1)}, bf16[256,512]{1,0:T(8,128)(2,1)S(1)}, u32[]{:S(2)}, u32[]{:S(2)}) %collective-permute-start.35) | collective-permute-done | bytes 262176 | tf_op jit(solution)/shard_map/ppermute | solution.py:32
  205.0 3.2 %collective-permute-start.36 = (bf16[528,512]{1,0:T(8,128)(2,1)S(1)}, bf16[528,512]{1,0:T(8,128)(2,1)S(1)}, u32[]{:S(2)}, u32[]{:S(2)}) collective-permute-start(bf16[528,512]{1,0:T(8,128)(2,1)S(1)} %pad_maximum_fusion.10), channel_id=1, source_target_pairs={{0,3},{1,0},{2,1},{3,2},{4,7},{5,4},{6,5},{7,6},{8,11},{9,8},{10,9... | collective-permute-start | bytes 1622024 | tf_op jit(solution)/shard_map/ppermute | solution.py:32
  208.5 6.9 %collective-permute-done.36 = bf16[528,512]{1,0:T(8,128)(2,1)S(1)} collective-permute-done((bf16[528,512]{1,0:T(8,128)(2,1)S(1)}, bf16[528,512]{1,0:T(8,128)(2,1)S(1)}, u32[]{:S(2)}, u32[]{:S(2)}) %collective-permute-start.36) | collective-permute-done | bytes 540704 | tf_op jit(solution)/shard_map/ppermute | solution.py:32
  215.4 3.6 %collective-permute-done.34 = bf16[528,512]{1,0:T(8,128)(2,1)S(1)} collective-permute-done((bf16[528,512]{1,0:T(8,128)(2,1)S(1)}, bf16[528,512]{1,0:T(8,128)(2,1)S(1)}, u32[]{:S(2)}, u32[]{:S(2)}) %collective-permute-start.34) | collective-permute-done | bytes 540704 | tf_op jit(solution)/shard_map/ppermute | solution.py:32
  219.0 1.1 add_convert_fusion.1
  (112 shorter events, 6.9 us)
Async XLA Ops:
  6.7 7.6 %collective-permute-start.10 = (bf16[2,64,512]{2,1,0:T(8,128)(2,1)S(1)}, bf16[2,64,512]{2,1,0:T(8,128)(2,1)S(1)}, u32[]{:S(2)}, u32[]{:S(2)}) collective-permute-start(bf16[2,64,512]{2,1,0:T(8,128)(2,1)S(1)} %get-tuple-element.32), channel_id=1, source_target_pairs={{0,64},{32,96},{64,128},{96,160},{128,192},{160,224},{192,0},{224,... | collective-permute-start | bytes 393224 | tf_op jit(solution)/shard_map/ppermute | solution.py:27
  11.0 5.0 %collective-permute-start.9 = (bf16[2,64,512]{2,1,0:T(8,128)(2,1)S(1)}, bf16[2,64,512]{2,1,0:T(8,128)(2,1)S(1)}, u32[]{:S(2)}, u32[]{:S(2)}) collective-permute-start(bf16[2,64,512]{2,1,0:T(8,128)(2,1)S(1)} %get-tuple-element.32), channel_id=1, source_target_pairs={{0,32},{32,64},{64,96},{96,128},{128,160},{160,192},{192,224},{224... | collective-permute-start | bytes 393224 | tf_op jit(solution)/shard_map/ppermute | solution.py:27
  16.0 6.8 %collective-permute-start.11 = (bf16[3,64,512]{2,1,0:T(8,128)(2,1)S(1)}, bf16[3,64,512]{2,1,0:T(8,128)(2,1)S(1)}, u32[]{:S(2)}, u32[]{:S(2)}) collective-permute-start(bf16[3,64,512]{2,1,0:T(8,128)(2,1)S(1)} %pad_maximum_fusion.15), channel_id=1, source_target_pairs={{0,64},{32,96},{64,128},{96,160},{128,192},{160,224},{192,0},{224,... | collective-permute-start | bytes 589832 | tf_op jit(solution)/shard_map/ppermute | solution.py:27
  22.9 16.0 %collective-permute-start.12 = (bf16[8,64,512]{2,1,0:T(8,128)(2,1)S(1)}, bf16[8,64,512]{2,1,0:T(8,128)(2,1)}, u32[]{:S(2)}, u32[]{:S(2)}) collective-permute-start(bf16[8,64,512]{2,1,0:T(8,128)(2,1)S(1)} %pad_maximum_fusion.11), channel_id=1, source_target_pairs={{0,4},{4,0},{1,5},{5,1},{2,6},{6,2},{3,7},{7,3},{8,12},{12,8},{9,1... | collective-permute-start | bytes 1572872 | tf_op jit(solution)/shard_map/ppermute | solution.py:20
  26.9 9.9 %collective-permute-start.24 = (bf16[4,64,512]{2,1,0:T(8,128)(2,1)S(1)}, bf16[4,64,512]{2,1,0:T(8,128)(2,1)S(1)}, u32[]{:S(2)}, u32[]{:S(2)}) collective-permute-start(bf16[4,64,512]{2,1,0:T(8,128)(2,1)S(1)} %get-tuple-element.28), channel_id=1, source_target_pairs={{0,8},{8,16},{16,24},{24,0},{4,28},{12,4},{20,12},{28,20},{1,9},{9... | collective-permute-start | bytes 786440 | tf_op jit(solution)/shard_map/ppermute | solution.py:27
  29.7 7.1 %collective-permute-start.25 = (bf16[2,64,512]{2,1,0:T(8,128)(2,1)S(1)}, bf16[2,64,512]{2,1,0:T(8,128)(2,1)S(1)}, u32[]{:S(2)}, u32[]{:S(2)}) collective-permute-start(bf16[2,64,512]{2,1,0:T(8,128)(2,1)S(1)} %dynamic-slice_bitcast_fusion), channel_id=1, source_target_pairs={{0,16},{8,24},{16,0},{24,8},{4,20},{12,28},{20,4},{28,12},{1,17},{... | collective-permute-start | bytes 393224 | tf_op jit(solution)/shard_map/ppermute | solution.py:27
  30.2 15.5 %collective-permute-start.1 = (bf16[2,64,512]{2,1,0:T(8,128)(2,1)}, bf16[2,64,512]{2,1,0:T(8,128)(2,1)}, u32[]{:S(2)}, u32[]{:S(2)}) collective-permute-start(bf16[2,64,512]{2,1,0:T(8,128)(2,1)} %get-tuple-element.31), channel_id=1, source_target_pairs={{0,8},{8,16},{16,24},{24,0},{4,28},{12,4},{20,12},{28,20},{1,9},{9... | collective-permute-start | bytes 393224 | tf_op jit(solution)/shard_map/ppermute | solution.py:27
  36.8 3.2 %copy-start.15 = (bf16[2,64,512]{2,1,0:T(8,128)(2,1)}, bf16[2,64,512]{2,1,0:T(8,128)(2,1)S(1)}, u32[]{:S(2)}) copy-start(bf16[2,64,512]{2,1,0:T(8,128)(2,1)S(1)} %collective-permute-done.25) | copy-start | bytes 393220
  36.9 23.0 %collective-permute-start.26 = (bf16[8,64,512]{2,1,0:T(8,128)(2,1)S(1)}, bf16[8,64,512]{2,1,0:T(8,128)(2,1)}, u32[]{:S(2)}, u32[]{:S(2)}) collective-permute-start(bf16[8,64,512]{2,1,0:T(8,128)(2,1)S(1)} %pad_maximum_fusion.12), channel_id=1, source_target_pairs={{0,4},{4,0},{1,5},{5,1},{2,6},{6,2},{3,7},{7,3},{8,12},{12,8},{9,1... | collective-permute-start | bytes 1572872 | tf_op jit(solution)/shard_map/ppermute | solution.py:20
  40.0 21.4 %copy-start.2 = (bf16[16,64,512]{2,1,0:T(8,128)(2,1)}, bf16[16,64,512]{2,1,0:T(8,128)(2,1)S(1)}, u32[]{:S(2)}) copy-start(bf16[16,64,512]{2,1,0:T(8,128)(2,1)S(1)} %pad_maximum_fusion.4.refs_11_) | copy-start | bytes 3145732
  40.0 29.2 %collective-permute-start.13 = (bf16[16,64,512]{2,1,0:T(8,128)(2,1)S(1)}, bf16[16,64,512]{2,1,0:T(8,128)(2,1)S(1)}, u32[]{:S(2)}, u32[]{:S(2)}) collective-permute-start(bf16[16,64,512]{2,1,0:T(8,128)(2,1)S(1)} %pad_maximum_fusion.4.refs_11_), channel_id=1, source_target_pairs={{0,8},{8,16},{16,24},{24,0},{4,28},{12,4},{20,12},{28,20},{1,9},{9... | collective-permute-start | bytes 3145736 | tf_op jit(solution)/shard_map/ppermute | solution.py:27
  40.4 5.3 %collective-permute-start.2 = (bf16[1,64,512]{2,1,0:T(8,128)(2,1)S(1)}, bf16[1,64,512]{2,1,0:T(8,128)(2,1)S(1)}, u32[]{:S(2)}, u32[]{:S(2)}) collective-permute-start(bf16[1,64,512]{2,1,0:T(8,128)(2,1)S(1)} %dynamic-slice_bitcast_fusion.2), channel_id=1, source_target_pairs={{0,16},{8,24},{16,0},{24,8},{4,20},{12,28},{20,4},{28,12},{1,17},{... | collective-permute-start | bytes 196616 | tf_op jit(solution)/shard_map/ppermute | solution.py:27
  41.1 18.8 %copy-start.16 = (bf16[2,64,512]{2,1,0:T(8,128)(2,1)S(1)}, bf16[2,64,512]{2,1,0:T(8,128)(2,1)}, u32[]{:S(2)}) copy-start(bf16[2,64,512]{2,1,0:T(8,128)(2,1)} %copy-done.15) | copy-start | bytes 393220
  46.6 22.5 %copy-start.19 = (s32[512]{0:T(512)S(1)}, s32[512]{0:T(512)}, u32[]{:S(2)}) copy-start(s32[512]{0:T(512)} %param.9) | copy-start | bytes 6148
  59.6 10.4 %copy-start.4 = (bf16[8,64,512]{2,1,0:T(8,128)(2,1)}, bf16[8,64,512]{2,1,0:T(8,128)(2,1)S(1)}, u32[]{:S(2)}) copy-start(bf16[8,64,512]{2,1,0:T(8,128)(2,1)S(1)} %all_gather.15.refs_4_) | copy-start | bytes 1572868
  59.6 12.1 %copy-start.11 = (bf16[512,512]{1,0:T(8,128)(2,1)S(1)}, bf16[512,512]{1,0:T(8,128)(2,1)}, u32[]{:S(2)}) copy-start(bf16[512,512]{1,0:T(8,128)(2,1)} %param.8) | copy-start | bytes 1572868
  59.7 8.3 %collective-permute-start.3 = (bf16[8,64,512]{2,1,0:T(8,128)(2,1)S(1)}, bf16[8,64,512]{2,1,0:T(8,128)(2,1)S(1)}, u32[]{:S(2)}, u32[]{:S(2)}) collective-permute-start(bf16[8,64,512]{2,1,0:T(8,128)(2,1)S(1)} %all_gather.15.refs_4_), channel_id=1, source_target_pairs={{0,32},{32,64},{64,96},{96,128},{128,160},{160,192},{192,224},{224... | collective-permute-start | bytes 1572872 | tf_op jit(solution)/shard_map/ppermute | solution.py:27
  61.4 24.8 %copy-start = (bf16[16,64,512]{2,1,0:T(8,128)(2,1)}, bf16[16,64,512]{2,1,0:T(8,128)(2,1)S(1)}, u32[]{:S(2)}) copy-start(bf16[16,64,512]{2,1,0:T(8,128)(2,1)S(1)} %maximum_select_fusion.refs_8_) | copy-start | bytes 3145732
  61.5 31.7 %collective-permute-start.27 = (bf16[16,64,512]{2,1,0:T(8,128)(2,1)S(1)}, bf16[16,64,512]{2,1,0:T(8,128)(2,1)}, u32[]{:S(2)}, u32[]{:S(2)}) collective-permute-start(bf16[16,64,512]{2,1,0:T(8,128)(2,1)S(1)} %maximum_select_fusion.refs_8_), channel_id=1, source_target_pairs={{0,32},{32,64},{64,96},{96,128},{128,160},{160,192},{192,224},{224... | collective-permute-start | bytes 3145736 | tf_op jit(solution)/shard_map/ppermute | solution.py:27
  68.0 18.2 %copy-start.6 = (bf16[8,64,512]{2,1,0:T(8,128)(2,1)}, bf16[8,64,512]{2,1,0:T(8,128)(2,1)S(1)}, u32[]{:S(2)}) copy-start(bf16[8,64,512]{2,1,0:T(8,128)(2,1)S(1)} %collective-permute-done.3.refs_5_) | copy-start | bytes 1572868
  68.0 17.1 %collective-permute-start.4 = (bf16[8,64,512]{2,1,0:T(8,128)(2,1)S(1)}, bf16[8,64,512]{2,1,0:T(8,128)(2,1)}, u32[]{:S(2)}, u32[]{:S(2)}) collective-permute-start(bf16[8,64,512]{2,1,0:T(8,128)(2,1)S(1)} %collective-permute-done.3.refs_5_), channel_id=1, source_target_pairs={{0,32},{32,64},{64,96},{96,128},{128,160},{160,192},{192,224},{224... | collective-permute-start | bytes 1572872 | tf_op jit(solution)/shard_map/ppermute | solution.py:27
  70.1 24.1 %collective-permute-start.14 = (bf16[8,64,512]{2,1,0:T(8,128)(2,1)}, bf16[8,64,512]{2,1,0:T(8,128)(2,1)}, u32[]{:S(2)}, u32[]{:S(2)}) collective-permute-start(bf16[8,64,512]{2,1,0:T(8,128)(2,1)} %slice.97), channel_id=1, source_target_pairs={{0,8},{8,16},{16,24},{24,0},{4,28},{12,4},{20,12},{28,20},{1,9},{9... | collective-permute-start | bytes 1572872 | tf_op jit(solution)/shard_map/ppermute | solution.py:27
  71.8 5.5 %collective-permute-start = (bf16[8,640]{1,0:T(8,128)(2,1)S(1)}, bf16[8,640]{1,0:T(8,128)(2,1)S(1)}, u32[]{:S(2)}, u32[]{:S(2)}) collective-permute-start(bf16[8,640]{1,0:T(8,128)(2,1)S(1)} %get-tuple-element.25), channel_id=1, source_target_pairs={{8,4},{16,12},{24,20},{32,28},{40,36},{48,44},{56,52},{64,60},{72,... | collective-permute-start | bytes 30728 | tf_op jit(solution)/shard_map/ppermute | solution.py:40
  85.0 11.9 %collective-permute-start.5 = (bf16[8,64,512]{2,1,0:T(8,128)(2,1)}, bf16[8,64,512]{2,1,0:T(8,128)(2,1)S(1)}, u32[]{:S(2)}, u32[]{:S(2)}) collective-permute-start(bf16[8,64,512]{2,1,0:T(8,128)(2,1)} %collective-permute-done.4.refs_6_), channel_id=1, source_target_pairs={{0,32},{32,64},{64,96},{96,128},{128,160},{160,192},{192,224},{224... | collective-permute-start | bytes 1572872 | tf_op jit(solution)/shard_map/ppermute | solution.py:27
  86.2 0.9 copy-start.13
  88.7 30.4 %all-to-all-start = ((bf16[4,528,512]{2,1,0:T(8,128)(2,1)}), bf16[4,528,512]{2,1,0:T(8,128)(2,1)}, u32[]{:S(2)}, u32[]{:S(2)}) async-start(bf16[4,528,512]{2,1,0:T(8,128)(2,1)} %broadcast_in_dim.14), calls=%async_computation | async-start | bytes 4325376 | tf_op jit(solution)/shard_map/all_to_all | solution.py:118
  93.2 6.8 %copy-start.7 = (bf16[8,64,512]{2,1,0:T(8,128)(2,1)S(1)}, bf16[8,64,512]{2,1,0:T(8,128)(2,1)}, u32[]{:S(2)}) copy-start(bf16[8,64,512]{2,1,0:T(8,128)(2,1)} %copy-done.6) | copy-start | bytes 1572868
  93.2 21.5 %collective-permute-start.28 = (bf16[16,64,512]{2,1,0:T(8,128)(2,1)}, bf16[16,64,512]{2,1,0:T(8,128)(2,1)}, u32[]{:S(2)}, u32[]{:S(2)}) collective-permute-start(bf16[16,64,512]{2,1,0:T(8,128)(2,1)} %collective-permute-done.27.refs_9_), channel_id=1, source_target_pairs={{0,32},{32,64},{64,96},{96,128},{128,160},{160,192},{192,224},{224... | collective-permute-start | bytes 3145736 | tf_op jit(solution)/shard_map/ppermute | solution.py:27
  96.5 22.6 %collective-permute-start.15 = (bf16[24,64,512]{2,1,0:T(8,128)(2,1)}, bf16[24,64,512]{2,1,0:T(8,128)(2,1)}, u32[]{:S(2)}, u32[]{:S(2)}) collective-permute-start(bf16[24,64,512]{2,1,0:T(8,128)(2,1)} %pad_maximum_fusion.1), channel_id=1, source_target_pairs={{0,4},{4,0},{1,5},{5,1},{2,6},{6,2},{3,7},{7,3},{8,12},{12,8},{9,1... | collective-permute-start | bytes 4718600 | tf_op jit(solution)/shard_map/ppermute | solution.py:20
  96.9 17.6 %copy-start.17 = (f32[2,2048]{1,0:T(2,128)S(1)}, f32[2,2048]{1,0:T(2,128)}, u32[]{:S(2)}) copy-start(f32[2,2048]{1,0:T(2,128)} %param.10) | copy-start | bytes 49156
  96.9 17.6 %copy-start.18 = (f32[2,3,512]{2,0,1:T(2,128)S(1)}, f32[2,3,512]{2,0,1:T(2,128)}, u32[]{:S(2)}) copy-start(f32[2,3,512]{2,0,1:T(2,128)} %param.14) | copy-start | bytes 36868
  97.0 13.4 %collective-permute-start.6 = (bf16[4,64,512]{2,1,0:T(8,128)(2,1)S(1)}, bf16[4,64,512]{2,1,0:T(8,128)(2,1)S(1)}, u32[]{:S(2)}, u32[]{:S(2)}) collective-permute-start(bf16[4,64,512]{2,1,0:T(8,128)(2,1)S(1)} %constant_dynamic-slice_fusion.2), channel_id=1, source_target_pairs={{0,32},{32,64},{64,96},{96,128},{128,160},{160,192},{192,224},{224... | collective-permute-start | bytes 786440 | tf_op jit(solution)/shard_map/ppermute | solution.py:27
  102.1 12.5 %copy-start.12 = (bf16[512,512]{1,0:T(8,128)(2,1)S(1)}, bf16[512,512]{1,0:T(8,128)(2,1)}, u32[]{:S(2)}) copy-start(bf16[512,512]{1,0:T(8,128)(2,1)} %param.8) | copy-start | bytes 1572868
  102.1 17.0 %copy-start.5 = (bf16[8,64,512]{2,1,0:T(8,128)(2,1)S(1)}, bf16[8,64,512]{2,1,0:T(8,128)(2,1)}, u32[]{:S(2)}) copy-start(bf16[8,64,512]{2,1,0:T(8,128)(2,1)} %copy-done.4) | copy-start | bytes 1572868
  102.1 17.0 %collective-permute-start.7 = (bf16[16,64,512]{2,1,0:T(8,128)(2,1)}, bf16[16,64,512]{2,1,0:T(8,128)(2,1)}, u32[]{:S(2)}, u32[]{:S(2)}) collective-permute-start(bf16[16,64,512]{2,1,0:T(8,128)(2,1)} %pad_maximum_fusion.3), channel_id=1, source_target_pairs={{0,4},{4,0},{1,5},{5,1},{2,6},{6,2},{3,7},{7,3},{8,12},{12,8},{9,1... | collective-permute-start | bytes 3145736 | tf_op jit(solution)/shard_map/ppermute | solution.py:20
  110.3 4.4 %copy-start.9 = (bf16[4,64,512]{2,1,0:T(8,128)(2,1)}, bf16[4,64,512]{2,1,0:T(8,128)(2,1)S(1)}, u32[]{:S(2)}) copy-start(bf16[4,64,512]{2,1,0:T(8,128)(2,1)S(1)} %collective-permute-done.6.refs_8_) | copy-start | bytes 786436
  111.3 7.8 %collective-permute-start.8 = (bf16[12,64,512]{2,1,0:T(8,128)(2,1)}, bf16[12,64,512]{2,1,0:T(8,128)(2,1)}, u32[]{:S(2)}, u32[]{:S(2)}) collective-permute-start(bf16[12,64,512]{2,1,0:T(8,128)(2,1)} %pad_maximum_fusion.5), channel_id=1, source_target_pairs={{0,4},{4,0},{1,5},{5,1},{2,6},{6,2},{3,7},{7,3},{8,12},{12,8},{9,1... | collective-permute-start | bytes 2359304 | tf_op jit(solution)/shard_map/ppermute | solution.py:20
  114.7 26.2 %collective-permute-start.29 = (bf16[16,64,512]{2,1,0:T(8,128)(2,1)}, bf16[16,64,512]{2,1,0:T(8,128)(2,1)S(1)}, u32[]{:S(2)}, u32[]{:S(2)}) collective-permute-start(bf16[16,64,512]{2,1,0:T(8,128)(2,1)} %collective-permute-done.28.refs_10_), channel_id=1, source_target_pairs={{0,32},{32,64},{64,96},{96,128},{128,160},{160,192},{192,224},{224... | collective-permute-start | bytes 3145736 | tf_op jit(solution)/shard_map/ppermute | solution.py:27
  119.2 1.2 copy-start.3
  120.4 1.0 copy-start.8
  121.4 0.9 copy-start.10
  135.7 6.9 %collective-permute-start.18 = (bf16[256,512]{1,0:T(8,128)(2,1)S(1)}, bf16[256,512]{1,0:T(8,128)(2,1)S(1)}, u32[]{:S(2)}, u32[]{:S(2)}) collective-permute-start(bf16[256,512]{1,0:T(8,128)(2,1)S(1)} %get-tuple-element.19), channel_id=1, source_target_pairs={{0,3},{1,0},{2,1},{3,2},{4,7},{5,4},{6,5},{7,6},{8,11},{9,8},{10,9... | collective-permute-start | bytes 786440 | tf_op jit(solution)/shard_map/ppermute | solution.py:32
  138.4 44.6 %collective-permute-start.31 = (bf16[32,64,512]{2,1,0:T(8,128)(2,1)S(1)}, bf16[32,64,512]{2,1,0:T(8,128)(2,1)S(1)}, u32[]{:S(2)}, u32[]{:S(2)}) collective-permute-start(bf16[32,64,512]{2,1,0:T(8,128)(2,1)S(1)} %pad_maximum_fusion), channel_id=1, source_target_pairs={{0,4},{4,0},{1,5},{5,1},{2,6},{6,2},{3,7},{7,3},{8,12},{12,8},{9,1... | collective-permute-start | bytes 6291464 | tf_op jit(solution)/shard_map/ppermute | solution.py:20
  141.0 10.9 %collective-permute-start.30 = (bf16[8,64,512]{2,1,0:T(8,128)(2,1)S(1)}, bf16[8,64,512]{2,1,0:T(8,128)(2,1)S(1)}, u32[]{:S(2)}, u32[]{:S(2)}) collective-permute-start(bf16[8,64,512]{2,1,0:T(8,128)(2,1)S(1)} %constant_dynamic-slice_fusion), channel_id=1, source_target_pairs={{0,32},{32,64},{64,96},{96,128},{128,160},{160,192},{192,224},{224... | collective-permute-start | bytes 1572872 | tf_op jit(solution)/shard_map/ppermute | solution.py:27
  142.0 9.7 %collective-permute-start.16 = (bf16[272,512]{1,0:T(8,128)(2,1)S(1)}, bf16[272,512]{1,0:T(8,128)(2,1)S(1)}, u32[]{:S(2)}, u32[]{:S(2)}) collective-permute-start(bf16[272,512]{1,0:T(8,128)(2,1)S(1)} %get-tuple-element.17), channel_id=1, source_target_pairs={{0,1},{1,2},{2,3},{3,0},{4,5},{5,6},{6,7},{7,4},{8,9},{9,10},{10,1... | collective-permute-start | bytes 835592 | tf_op jit(solution)/shard_map/ppermute | solution.py:32
  142.7 12.2 %collective-permute-start.19 = (bf16[528,512]{1,0:T(8,128)(2,1)S(1)}, bf16[528,512]{1,0:T(8,128)(2,1)S(1)}, u32[]{:S(2)}, u32[]{:S(2)}) collective-permute-start(bf16[528,512]{1,0:T(8,128)(2,1)S(1)} %pad_maximum_fusion.8), channel_id=1, source_target_pairs={{0,3},{1,0},{2,1},{3,2},{4,7},{5,4},{6,5},{7,6},{8,11},{9,8},{10,9... | collective-permute-start | bytes 1622024 | tf_op jit(solution)/shard_map/ppermute | solution.py:32
  151.8 14.5 %copy-start.14 = (bf16[528,640]{1,0:T(8,128)(2,1)S(1)}, bf16[528,640]{1,0:T(8,128)(2,1)}, u32[]{:S(2)}) copy-start(bf16[528,640]{1,0:T(8,128)(2,1)} %copy-done.13) | copy-start | bytes 2027524
  151.8 14.5 %collective-permute-start.17 = (bf16[528,512]{1,0:T(8,128)(2,1)S(1)}, bf16[528,512]{1,0:T(8,128)(2,1)S(1)}, u32[]{:S(2)}, u32[]{:S(2)}) collective-permute-start(bf16[528,512]{1,0:T(8,128)(2,1)S(1)} %pad_maximum_fusion.7), channel_id=1, source_target_pairs={{0,1},{1,2},{2,3},{3,0},{4,5},{5,6},{6,7},{7,4},{8,9},{9,10},{10,1... | collective-permute-start | bytes 1622024 | tf_op jit(solution)/shard_map/ppermute | solution.py:32
  152.1 35.3 %collective-permute-start.32 = (bf16[24,64,512]{2,1,0:T(8,128)(2,1)S(1)}, bf16[24,64,512]{2,1,0:T(8,128)(2,1)S(1)}, u32[]{:S(2)}, u32[]{:S(2)}) collective-permute-start(bf16[24,64,512]{2,1,0:T(8,128)(2,1)S(1)} %pad_maximum_fusion.2), channel_id=1, source_target_pairs={{0,4},{4,0},{1,5},{5,1},{2,6},{6,2},{3,7},{7,3},{8,12},{12,8},{9,1... | collective-permute-start | bytes 4718600 | tf_op jit(solution)/shard_map/ppermute | solution.py:20
  166.3 21.1 %copy-start.1 = (bf16[16,64,512]{2,1,0:T(8,128)(2,1)S(1)}, bf16[16,64,512]{2,1,0:T(8,128)(2,1)}, u32[]{:S(2)}) copy-start(bf16[16,64,512]{2,1,0:T(8,128)(2,1)} %copy-done) | copy-start | bytes 3145732
  166.6 13.6 %collective-permute-start.20 = (bf16[528,512]{1,0:T(8,128)(2,1)S(1)}, bf16[528,512]{1,0:T(8,128)(2,1)S(1)}, u32[]{:S(2)}, u32[]{:S(2)}) collective-permute-start(bf16[528,512]{1,0:T(8,128)(2,1)S(1)} %add_convert_fusion.refs_0_), channel_id=1, source_target_pairs={{0,1},{1,2},{2,3},{3,0},{4,5},{5,6},{6,7},{7,4},{8,9},{9,10},{10,1... | collective-permute-start | bytes 1622024 | tf_op jit(solution)/shard_map/ppermute | solution.py:32
  166.7 13.6 %collective-permute-start.21 = (bf16[528,512]{1,0:T(8,128)(2,1)S(1)}, bf16[528,512]{1,0:T(8,128)(2,1)S(1)}, u32[]{:S(2)}, u32[]{:S(2)}) collective-permute-start(bf16[528,512]{1,0:T(8,128)(2,1)S(1)} %add_convert_fusion.refs_0_), channel_id=1, source_target_pairs={{0,3},{1,0},{2,1},{3,2},{4,7},{5,4},{6,5},{7,6},{8,11},{9,8},{10,9... | collective-permute-start | bytes 1622024 | tf_op jit(solution)/shard_map/ppermute | solution.py:32
  180.2 7.1 %collective-permute-start.22 = (bf16[272,512]{1,0:T(8,128)(2,1)S(1)}, bf16[272,512]{1,0:T(8,128)(2,1)S(1)}, u32[]{:S(2)}, u32[]{:S(2)}) collective-permute-start(bf16[272,512]{1,0:T(8,128)(2,1)S(1)} %slice.98), channel_id=1, source_target_pairs={{0,1},{1,2},{2,3},{3,0},{4,5},{5,6},{6,7},{7,4},{8,9},{9,10},{10,1... | collective-permute-start | bytes 835592 | tf_op jit(solution)/shard_map/ppermute | solution.py:32
  180.3 6.0 %collective-permute-start.23 = (bf16[256,512]{1,0:T(8,128)(2,1)S(1)}, bf16[256,512]{1,0:T(8,128)(2,1)S(1)}, u32[]{:S(2)}, u32[]{:S(2)}) collective-permute-start(bf16[256,512]{1,0:T(8,128)(2,1)S(1)} %slice.99), channel_id=1, source_target_pairs={{0,3},{1,0},{2,1},{3,2},{4,7},{5,4},{6,5},{7,6},{8,11},{9,8},{10,9... | collective-permute-start | bytes 786440 | tf_op jit(solution)/shard_map/ppermute | solution.py:32
  199.3 5.6 %collective-permute-start.35 = (bf16[256,512]{1,0:T(8,128)(2,1)S(1)}, bf16[256,512]{1,0:T(8,128)(2,1)S(1)}, u32[]{:S(2)}, u32[]{:S(2)}) collective-permute-start(bf16[256,512]{1,0:T(8,128)(2,1)S(1)} %get-tuple-element.24), channel_id=1, source_target_pairs={{0,3},{1,0},{2,1},{3,2},{4,7},{5,4},{6,5},{7,6},{8,11},{9,8},{10,9... | collective-permute-start | bytes 786440 | tf_op jit(solution)/shard_map/ppermute | solution.py:32
  201.6 6.7 %collective-permute-start.33 = (bf16[272,512]{1,0:T(8,128)(2,1)S(1)}, bf16[272,512]{1,0:T(8,128)(2,1)S(1)}, u32[]{:S(2)}, u32[]{:S(2)}) collective-permute-start(bf16[272,512]{1,0:T(8,128)(2,1)S(1)} %get-tuple-element.22), channel_id=1, source_target_pairs={{0,1},{1,2},{2,3},{3,0},{4,5},{5,6},{6,7},{7,4},{8,9},{9,10},{10,1... | collective-permute-start | bytes 835592 | tf_op jit(solution)/shard_map/ppermute | solution.py:32
  205.0 10.5 %collective-permute-start.36 = (bf16[528,512]{1,0:T(8,128)(2,1)S(1)}, bf16[528,512]{1,0:T(8,128)(2,1)S(1)}, u32[]{:S(2)}, u32[]{:S(2)}) collective-permute-start(bf16[528,512]{1,0:T(8,128)(2,1)S(1)} %pad_maximum_fusion.10), channel_id=1, source_target_pairs={{0,3},{1,0},{2,1},{3,2},{4,7},{5,4},{6,5},{7,6},{8,11},{9,8},{10,9... | collective-permute-start | bytes 1622024 | tf_op jit(solution)/shard_map/ppermute | solution.py:32
  208.4 10.6 %collective-permute-start.34 = (bf16[528,512]{1,0:T(8,128)(2,1)S(1)}, bf16[528,512]{1,0:T(8,128)(2,1)S(1)}, u32[]{:S(2)}, u32[]{:S(2)}) collective-permute-start(bf16[528,512]{1,0:T(8,128)(2,1)S(1)} %pad_maximum_fusion.9), channel_id=1, source_target_pairs={{0,1},{1,2},{2,3},{3,0},{4,5},{5,6},{6,7},{7,4},{8,9},{9,10},{10,1... | collective-permute-start | bytes 1622024 | tf_op jit(solution)/shard_map/ppermute | solution.py:32
where the time goes:
time: 224 us; the launch traced here: 220 us
  waiting for transfers between devices  92.4 us (41%)
  starting transfers between devices  60 us (27%)
  Pallas kernels  25.3 us (11%)
  blocking collectives  19.8 us (9%)
  other arithmetic  14.1 us (6%)
  local copies, waits for them, and re-layouts  7.84 us (4%)
    ppermute x12, waiting for transfers between devices, shifted(): lax.ppermute(value, axis, [(i, (i + step) % size) for i in range(size)])  49 us
    ppermute x17, waiting for transfers between devices, onward(): return lax.ppermute(value, (axis, 'c'), pairs)  39.8 us
    ppermute x17, starting transfers between devices, onward(): return lax.ppermute(value, (axis, 'c'), pairs)  25.3 us
    pallas_call x2, Pallas kernels, layer(): pl.pallas_call(functools.partial(layer_kernel, index, cut, len(sources),...  25.3 us
    ppermute x12, starting transfers between devices, shifted(): lax.ppermute(value, axis, [(i, (i + step) % size) for i in range(size)])  15.3 us
    all_gather x1, blocking collectives, by_y_then_z(): around = lax.all_gather(mixed, 'c', axis=0, tiled=True)  13 us
    ppermute x7, starting transfers between devices, partner(): return lax.ppermute(value, 'c', [(0, 1), (1, 0)])  12.8 us
    all_gather x1, blocking collectives, per_device(): chip = lax.all_gather(mats, 'c', axis=2, tiled=True)  5.01 us
  transfers between devices with their start and end apart: 38, of which 20 were waited for; matrix products, arithmetic and copies ran while one was open for 7% of the time, Pallas kernels for 6%

commit v1 on v0

--- a/solution.py
+++ b/solution.py
@@ -13,7 +13,7 @@
 NZ, NY, NC, NX = 8, 4, 2, 4
 SP = ("z", "y", "c")
 HALO = 8
-VMEM_LIMIT = 26
+VMEM_LIMIT = 22
 
 
 def partner(value):
@@ -55,13 +55,22 @@
     if own.shape[0] == 2:
         around = lax.all_gather(mixed, "c", axis=0, tiled=True)
     else:
+        mixed = lax.optimization_barrier(mixed)
         other = partner(mixed)
-        around = jnp.where(c == 0, jnp.concatenate([mixed, other]), jnp.concatenate([other, mixed]))
+        around = jnp.concatenate([other, mixed], axis=0)
     moved = [around]
     for _ in range(3):
         moved.append(onward(moved[-1], "z"))
-    moved = moved[1:] + [onward(half(moved[-1], c), "z")]
-    return [around] + moved + [partner(jnp.concatenate(moved[k : k + 2], axis=0)) for k in (0, 2)]
+    last = half(moved[-1], c) if own.shape[0] == 2 else moved[-1][mixed.shape[0] :]
+    moved = moved[1:] + [onward(last, "z")]
+    if own.shape[0] == 2:
+        swapped = [partner(jnp.concatenate(moved[:2], axis=0))]
+        swapped += [partner(moved[2]), partner(moved[3])]
+    else:
+        swapped = []
+        for k in (0, 2):
+            swapped.append(partner(jnp.concatenate(moved[k : k + 2], axis=0)))
+    return [around] + moved + swapped
 
 
 def by_z_then_y(own, c):
@@ -70,10 +79,12 @@
     far = onward(jnp.concatenate([one, half(two, c)], axis=0), "z", 2)
     side = jnp.concatenate([half(own, c), one, two, far], axis=0)
     side = lax.optimization_barrier(side)
-    around = jnp.concatenate([partner(side), side], axis=0)
+    other = partner(side)
+    around = jnp.concatenate([other, side], axis=0)
     near = onward(around, "y")
     moved = [near, onward(near[near.shape[0] // 2 :], "y")]
-    return [around] + moved + [partner(jnp.concatenate(moved, axis=0))]
+    swapped = partner(jnp.concatenate(moved, axis=0))
+    return [around] + moved + [swapped]
 
 
 def units_of(layer_index, y, z, c, s):
@@ -90,15 +101,17 @@
         near = [(m, s) for m in range(2 * count)]
         return [(m, 0) for m in halves] + near + [(m, 2) for m in halves]
 
-    both = mixed(0, -1) + mixed(1, 1)
+    def both(c, s):
+        return mixed(0, -1) + mixed(1, 1) if layer_index == 0 else mixed(1 - c, -s) + mixed(c, s)
 
     def moved_a(c, s):
-        return [a(both, k * s) for k in (1, 2, 3)] + [a(mixed(c, s), 4)]
+        return [a(both(c, s), k * s) for k in (1, 2, 3)] + [a(mixed(c, s), 4)]
 
     theirs = moved_a(1 - c, -s)
-    first = [a(both, 0)] + moved_a(c, s) + [theirs[0] + theirs[1], theirs[2] + theirs[3]]
+    first = [a(both(c, s), 0)] + moved_a(c, s) + [theirs[0] + theirs[1]]
     if layer_index == 1:
-        return first
+        return first + [theirs[2] + theirs[3]]
+    first += theirs[2:]
 
     def side(c, s):
         return [(2 + c, 0)] + [(m, k * s) for k in (1, 2, 3) for m in (2, 3)] + [(2 + c, 4)]
@@ -121,7 +134,9 @@
 def gather_x(rows, cut):
     left = shifted(rows, "x", 1)
     right = shifted(rows, "x", -1)
-    return [rows, left, right, shifted(left[:cut], "x", 1), shifted(right[cut:], "x", -1)]
+    far_top = shifted(left[:cut], "x", 1)
+    far_bottom = shifted(right[cut:], "x", -1)
+    return [rows, left, right, far_top, far_bottom]
 
 
 def wide(value):

time: 224 us -> 216 us (0.964)
  blocking collectives: 19.8 us -> 11.6 us
  other arithmetic: 14.1 us -> 8.8 us
  waiting for transfers between devices: 92.4 us -> 95.1 us
  starting transfers between devices: 60 us -> 62.3 us
    all_gather x1, blocking collectives: 13 us -> 4.78 us  [by_y_then_z(): around = lax.all_gather(mixed, 'c', axis=0, tiled=True)]
    ppermute x17, waiting for transfers between devices: 39.8 us -> 44 us  [onward(): return lax.ppermute(value, (axis, 'c'), pairs)]
    concatenate x6, other arithmetic: 8.43 us -> 5.51 us  [the longest x1 2.17 us: by_y_then_z(): swapped = [partner(jnp.concatenate(moved[:2], axis=0))]]
    ppermute x12, starting transfers between devices: 15.3 us -> 17.6 us  [shifted(): lax.ppermute(value, axis, [(i, (i + step) % size) for i in range(size)])]
    ppermute x7 -> x8, starting transfers between devices: 12.8 us -> 13.3 us  [partner(): return lax.ppermute(value, 'c', [(0, 1), (1, 0)])]
  transfers between devices with their start and end apart: 38 -> 39, of which waited for: 20 -> 23; matrix products, arithmetic and copies ran while one was open for 7% -> 5% of each run, Pallas kernels for 6% -> 6%
where the time goes in v1:
time: 216 us; the launch traced here: 213 us
  waiting for transfers between devices  95.1 us (44%)
  starting transfers between devices  62.3 us (29%)
  Pallas kernels  25.5 us (12%)
  blocking collectives  11.6 us (5%)
  local copies, waits for them, and re-layouts  9.53 us (4%)
  other arithmetic  8.8 us (4%)
    ppermute x12, waiting for transfers between devices, shifted(): lax.ppermute(value, axis, [(i, (i + step) % size) for i in range(size)])  49.9 us
    ppermute x17, waiting for transfers between devices, onward(): return lax.ppermute(value, (axis, 'c'), pairs)  44 us
    pallas_call x2, Pallas kernels, layer(): pl.pallas_call(functools.partial(layer_kernel, index, cut, len(sources),...  25.5 us
    ppermute x17, starting transfers between devices, onward(): return lax.ppermute(value, (axis, 'c'), pairs)  25.1 us
    ppermute x12, starting transfers between devices, shifted(): lax.ppermute(value, axis, [(i, (i + step) % size) for i in range(size)])  17.6 us
    ppermute x8, starting transfers between devices, partner(): return lax.ppermute(value, 'c', [(0, 1), (1, 0)])  13.3 us
    all_gather x1, blocking collectives, per_device(): chip = lax.all_gather(mats, 'c', axis=2, tiled=True)  5.01 us
    all_gather x1, blocking collectives, by_y_then_z(): around = lax.all_gather(mixed, 'c', axis=0, tiled=True)  4.78 us
  transfers between devices with their start and end apart: 39, of which 23 were waited for; matrix products, arithmetic and copies ran while one was open for 5% of the time, Pallas kernels for 6%

profile of v1, /device:TPU:1, one launch (start us, length us, event | category | flops | bytes accessed | tf_op | source)
XLA Modules:
  0.0 213.4 jit_solution(914975647032652730)
XLA Ops:
  0.0 1.0 pad_maximum_fusion.13
  1.0 5.0 %all_gather.14 = bf16[2,4,64,512]{3,2,1,0:T(8,128)(2,1)S(1)} all-gather(bf16[2,4,32,512]{3,2,1,0:T(8,128)(2,1)S(1)} %pad_maximum_fusion.13), channel_id=1, replica_groups=mesh['z'=8,'y'=4,'c'=2,'x'=4] {'c'}, dimensions={2}, use_global_device_ids=true | all-gather | bytes 786432 | tf_op jit(solution)/shard_map/all_gather | solution.py:262
  6.0 0.7 fusion.7
  6.7 4.3 %collective-permute-start.11 = (bf16[2,64,512]{2,1,0:T(8,128)(2,1)S(1)}, bf16[2,64,512]{2,1,0:T(8,128)(2,1)S(1)}, u32[]{:S(2)}, u32[]{:S(2)}) collective-permute-start(bf16[2,64,512]{2,1,0:T(8,128)(2,1)S(1)} %get-tuple-element.32), channel_id=1, source_target_pairs={{0,64},{32,96},{64,128},{96,160},{128,192},{160,224},{192,0},{224,... | collective-permute-start | bytes 393224 | tf_op jit(solution)/shard_map/ppermute | solution.py:27
  11.0 0.7 collective-permute-start.10
  11.7 2.6 %collective-permute-done.11 = bf16[2,64,512]{2,1,0:T(8,128)(2,1)S(1)} collective-permute-done((bf16[2,64,512]{2,1,0:T(8,128)(2,1)S(1)}, bf16[2,64,512]{2,1,0:T(8,128)(2,1)S(1)}, u32[]{:S(2)}, u32[]{:S(2)}) %collective-permute-start.11) | collective-permute-done | bytes 131104 | tf_op jit(solution)/shard_map/ppermute | solution.py:27
  14.3 1.6 collective-permute-done.10
  16.0 2.5 %collective-permute-start.12 = (bf16[3,64,512]{2,1,0:T(8,128)(2,1)S(1)}, bf16[3,64,512]{2,1,0:T(8,128)(2,1)S(1)}, u32[]{:S(2)}, u32[]{:S(2)}) collective-permute-start(bf16[3,64,512]{2,1,0:T(8,128)(2,1)S(1)} %pad_maximum_fusion.15), channel_id=1, source_target_pairs={{0,64},{32,96},{64,128},{96,160},{128,192},{160,224},{192,0},{224,... | collective-permute-start | bytes 589832 | tf_op jit(solution)/shard_map/ppermute | solution.py:27
  18.4 4.3 %collective-permute-done.12 = bf16[3,64,512]{2,1,0:T(8,128)(2,1)S(1)} collective-permute-done((bf16[3,64,512]{2,1,0:T(8,128)(2,1)S(1)}, bf16[3,64,512]{2,1,0:T(8,128)(2,1)S(1)}, u32[]{:S(2)}, u32[]{:S(2)}) %collective-permute-start.12) | collective-permute-done | bytes 196640 | tf_op jit(solution)/shard_map/ppermute | solution.py:27
  22.9 4.0 %collective-permute-start.13 = (bf16[8,64,512]{2,1,0:T(8,128)(2,1)S(1)}, bf16[8,64,512]{2,1,0:T(8,128)(2,1)S(1)}, u32[]{:S(2)}, u32[]{:S(2)}) collective-permute-start(bf16[8,64,512]{2,1,0:T(8,128)(2,1)S(1)} %pad_maximum_fusion.11), channel_id=1, source_target_pairs={{0,4},{4,0},{1,5},{5,1},{2,6},{6,2},{3,7},{7,3},{8,12},{12,8},{9,1... | collective-permute-start | bytes 1572872 | tf_op jit(solution)/shard_map/ppermute | solution.py:20
  26.9 2.8 %collective-permute-start.25 = (bf16[4,64,512]{2,1,0:T(8,128)(2,1)S(1)}, bf16[4,64,512]{2,1,0:T(8,128)(2,1)S(1)}, u32[]{:S(2)}, u32[]{:S(2)}) collective-permute-start(bf16[4,64,512]{2,1,0:T(8,128)(2,1)S(1)} %get-tuple-element.28), channel_id=1, source_target_pairs={{0,8},{8,16},{16,24},{24,0},{4,28},{12,4},{20,12},{28,20},{1,9},{9... | collective-permute-start | bytes 786440 | tf_op jit(solution)/shard_map/ppermute | solution.py:27
  30.3 1.0 collective-permute-start.14
  31.3 5.5 %collective-permute-done.26 = bf16[2,64,512]{2,1,0:T(8,128)(2,1)S(1)} collective-permute-done((bf16[2,64,512]{2,1,0:T(8,128)(2,1)S(1)}, bf16[2,64,512]{2,1,0:T(8,128)(2,1)S(1)}, u32[]{:S(2)}, u32[]{:S(2)}) %collective-permute-start.26) | collective-permute-done | bytes 131104 | tf_op jit(solution)/shard_map/ppermute | solution.py:27
  36.9 2.0 collective-permute-start.27
  39.2 0.7 collective-permute-start.2
  39.9 4.6 %collective-permute-done.2 = bf16[1,64,512]{2,1,0:T(8,128)(2,1)S(1)} collective-permute-done((bf16[1,64,512]{2,1,0:T(8,128)(2,1)S(1)}, bf16[1,64,512]{2,1,0:T(8,128)(2,1)S(1)}, u32[]{:S(2)}, u32[]{:S(2)}) %collective-permute-start.2) | collective-permute-done | bytes 65568 | tf_op jit(solution)/shard_map/ppermute | solution.py:27
  44.5 5.3 %collective-permute-done.1 = bf16[2,64,512]{2,1,0:T(8,128)(2,1)S(1)} collective-permute-done((bf16[2,64,512]{2,1,0:T(8,128)(2,1)S(1)}, bf16[2,64,512]{2,1,0:T(8,128)(2,1)S(1)}, u32[]{:S(2)}, u32[]{:S(2)}) %collective-permute-start.1) | collective-permute-done | bytes 131104 | tf_op jit(solution)/shard_map/ppermute | solution.py:27
  49.9 4.8 %all_gather.15.refs_4_ = bf16[8,64,512]{2,1,0:T(8,128)(2,1)} all-gather(bf16[4,64,512]{2,1,0:T(8,128)(2,1)S(1)} %pad_maximum_fusion.14), channel_id=1, replica_groups=mesh['z'=8,'y'=4,'c'=2,'x'=4] {'c'}, dimensions={0}, use_global_device_ids=true | all-gather | bytes 786432 | tf_op jit(solution)/shard_map/all_gather | solution.py:56
  54.7 0.8 collective-permute-start.3
  55.6 1.3 collective-permute-start.28
  56.9 0.8 slice.101
  58.6 1.9 collective-permute-start
  60.5 1.8 all-gather
  62.4 1.0 collective-permute-done.3.refs_5_
  63.4 1.9 collective-permute-start.4
  65.3 0.8 copy-done.8
  66.2 1.5 broadcast_in_dim.14
  67.8 4.5 %all-to-all-start = ((bf16[4,528,512]{2,1,0:T(8,128)(2,1)}), bf16[4,528,512]{2,1,0:T(8,128)(2,1)}, u32[]{:S(2)}, u32[]{:S(2)}) async-start(bf16[4,528,512]{2,1,0:T(8,128)(2,1)} %broadcast_in_dim.14), calls=%async_computation | async-start | bytes 4325376 | tf_op jit(solution)/shard_map/all_to_all | solution.py:131
  72.3 1.3 pad_maximum_fusion.1
  74.7 2.4 %collective-permute-start.29 = (bf16[16,64,512]{2,1,0:T(8,128)(2,1)}, bf16[16,64,512]{2,1,0:T(8,128)(2,1)}, u32[]{:S(2)}, u32[]{:S(2)}) collective-permute-start(bf16[16,64,512]{2,1,0:T(8,128)(2,1)} %collective-permute-done.28.refs_9_), channel_id=1, source_target_pairs={{0,32},{32,64},{64,96},{96,128},{128,160},{160,192},{192,224},{224... | collective-permute-start | bytes 3145736 | tf_op jit(solution)/shard_map/ppermute | solution.py:27
  77.1 3.2 %collective-permute-done.4.refs_6_ = bf16[8,64,512]{2,1,0:T(8,128)(2,1)S(1)} collective-permute-done((bf16[8,64,512]{2,1,0:T(8,128)(2,1)}, bf16[8,64,512]{2,1,0:T(8,128)(2,1)S(1)}, u32[]{:S(2)}, u32[]{:S(2)}) %collective-permute-start.4) | collective-permute-done | bytes 524320 | tf_op jit(solution)/shard_map/ppermute | solution.py:27
  80.3 1.9 collective-permute-start.5
  82.2 2.2 %pad_maximum_fusion.3 = bf16[16,64,512]{2,1,0:T(8,128)(2,1)} fusion(bf16[8,64,512]{2,1,0:T(8,128)(2,1)S(1)} %collective-permute-done.4.refs_6_, bf16[8,64,512]{2,1,0:T(8,128)(2,1)} %collective-permute-done.3.refs_5_), kind=kLoop, calls=%fused_computation.4 | loop fusion | flops 524288 | bytes 2097152 | tf_op jit(solution)/shard_map/concatenate | solution.py:67
  84.9 12.3 %collective-permute-done.5.refs_7_ = bf16[8,64,512]{2,1,0:T(8,128)(2,1)} collective-permute-done((bf16[8,64,512]{2,1,0:T(8,128)(2,1)S(1)}, bf16[8,64,512]{2,1,0:T(8,128)(2,1)}, u32[]{:S(2)}, u32[]{:S(2)}) %collective-permute-start.5) | collective-permute-done | bytes 524320 | tf_op jit(solution)/shard_map/ppermute | solution.py:27
  97.2 1.7 constant_dynamic-slice_fusion.1
  98.8 1.9 collective-permute-start.6
  101.5 2.9 %collective-permute-done.6.refs_8_ = bf16[4,64,512]{2,1,0:T(8,128)(2,1)} collective-permute-done((bf16[4,64,512]{2,1,0:T(8,128)(2,1)}, bf16[4,64,512]{2,1,0:T(8,128)(2,1)}, u32[]{:S(2)}, u32[]{:S(2)}) %collective-permute-start.6) | collective-permute-done | bytes 262176 | tf_op jit(solution)/shard_map/ppermute | solution.py:27
  104.4 4.7 %collective-permute-start.9 = (bf16[4,64,512]{2,1,0:T(8,128)(2,1)}, bf16[4,64,512]{2,1,0:T(8,128)(2,1)}, u32[]{:S(2)}, u32[]{:S(2)}) collective-permute-start(bf16[4,64,512]{2,1,0:T(8,128)(2,1)} %collective-permute-done.6.refs_8_), channel_id=1, source_target_pairs={{0,4},{4,0},{1,5},{5,1},{2,6},{6,2},{3,7},{7,3},{8,12},{12,8},{9,1... | collective-permute-start | bytes 786440 | tf_op jit(solution)/shard_map/ppermute | solution.py:20
  109.4 1.1 collective-permute-done.9.refs_11_
  110.6 1.2 copy-done.1
  111.8 1.0 copy-done.3
  112.8 1.0 copy-done.5
  113.9 13.6 %shard_map.82 = (bf16[528,512]{1,0:T(8,128)(2,1)S(1)}, bf16[528,512]{1,0:T(8,128)(2,1)S(1)}, bf16[528,512]{1,0:T(8,128)(2,1)S(1)}, bf16[272,512]{1,0:T(8,128)(2,1)S(1)}, bf16[256,512]{1,0:T(8,128)(2,1)S(1)}) custom-call(bf16[4,528,512]{2,1,0:T(8,128)(2,1)} %all-to-all-done.refs_0_, f32[2,4,512]{2,1,0:T(4,128)S(1)} %reshape.9.refs_1_.refs_5_, ...), custom_call_target="tpu_custom_call" | custom-call | flops 4429185024 | bytes 8388608 | tf_op jit(solution)/shard_map/pallas_call | solution.py:244
  127.5 2.5 %collective-permute-start.19 = (bf16[256,512]{1,0:T(8,128)(2,1)S(1)}, bf16[256,512]{1,0:T(8,128)(2,1)S(1)}, u32[]{:S(2)}, u32[]{:S(2)}) collective-permute-start(bf16[256,512]{1,0:T(8,128)(2,1)S(1)} %get-tuple-element.19), channel_id=1, source_target_pairs={{0,3},{1,0},{2,1},{3,2},{4,7},{5,4},{6,5},{7,6},{8,11},{9,8},{10,9... | collective-permute-start | bytes 786440 | tf_op jit(solution)/shard_map/ppermute | solution.py:32
  130.0 1.7 pad_maximum_fusion
  131.7 0.7 collective-permute-start.32
  132.5 1.6 collective-permute-start.31
  134.2 1.1 collective-permute-done.19
  135.4 3.5 %collective-permute-start.20 = (bf16[528,512]{1,0:T(8,128)(2,1)S(1)}, bf16[528,512]{1,0:T(8,128)(2,1)S(1)}, u32[]{:S(2)}, u32[]{:S(2)}) collective-permute-start(bf16[528,512]{1,0:T(8,128)(2,1)S(1)} %pad_maximum_fusion.8), channel_id=1, source_target_pairs={{0,3},{1,0},{2,1},{3,2},{4,7},{5,4},{6,5},{7,6},{8,11},{9,8},{10,9... | collective-permute-start | bytes 1622024 | tf_op jit(solution)/shard_map/ppermute | solution.py:32
  138.9 4.4 %collective-permute-done.17 = bf16[272,512]{1,0:T(8,128)(2,1)S(1)} collective-permute-done((bf16[272,512]{1,0:T(8,128)(2,1)S(1)}, bf16[272,512]{1,0:T(8,128)(2,1)S(1)}, u32[]{:S(2)}, u32[]{:S(2)}) %collective-permute-start.17) | collective-permute-done | bytes 278560 | tf_op jit(solution)/shard_map/ppermute | solution.py:32
  144.1 5.2 %collective-permute-done.20 = bf16[528,512]{1,0:T(8,128)(2,1)S(1)} collective-permute-done((bf16[528,512]{1,0:T(8,128)(2,1)S(1)}, bf16[528,512]{1,0:T(8,128)(2,1)S(1)}, u32[]{:S(2)}, u32[]{:S(2)}) %collective-permute-start.20) | collective-permute-done | bytes 540704 | tf_op jit(solution)/shard_map/ppermute | solution.py:32
  149.3 9.2 %collective-permute-done.18 = bf16[528,512]{1,0:T(8,128)(2,1)S(1)} collective-permute-done((bf16[528,512]{1,0:T(8,128)(2,1)S(1)}, bf16[528,512]{1,0:T(8,128)(2,1)S(1)}, u32[]{:S(2)}, u32[]{:S(2)}) %collective-permute-start.18) | collective-permute-done | bytes 540704 | tf_op jit(solution)/shard_map/ppermute | solution.py:32
  158.9 2.7 %collective-permute-start.22 = (bf16[528,512]{1,0:T(8,128)(2,1)S(1)}, bf16[528,512]{1,0:T(8,128)(2,1)S(1)}, u32[]{:S(2)}, u32[]{:S(2)}) collective-permute-start(bf16[528,512]{1,0:T(8,128)(2,1)S(1)} %add_convert_fusion.refs_0_), channel_id=1, source_target_pairs={{0,3},{1,0},{2,1},{3,2},{4,7},{5,4},{6,5},{7,6},{8,11},{9,8},{10,9... | collective-permute-start | bytes 1622024 | tf_op jit(solution)/shard_map/ppermute | solution.py:32
  161.6 11.3 %collective-permute-done.21.refs_1_ = bf16[528,512]{1,0:T(8,128)(2,1)S(1)} collective-permute-done((bf16[528,512]{1,0:T(8,128)(2,1)S(1)}, bf16[528,512]{1,0:T(8,128)(2,1)S(1)}, u32[]{:S(2)}, u32[]{:S(2)}) %collective-permute-start.21) | collective-permute-done | bytes 540704 | tf_op jit(solution)/shard_map/ppermute | solution.py:32
  173.1 2.7 %collective-permute-start.24 = (bf16[256,512]{1,0:T(8,128)(2,1)S(1)}, bf16[256,512]{1,0:T(8,128)(2,1)S(1)}, u32[]{:S(2)}, u32[]{:S(2)}) collective-permute-start(bf16[256,512]{1,0:T(8,128)(2,1)S(1)} %slice.103), channel_id=1, source_target_pairs={{0,3},{1,0},{2,1},{3,2},{4,7},{5,4},{6,5},{7,6},{8,11},{9,8},{10,9... | collective-permute-start | bytes 786440 | tf_op jit(solution)/shard_map/ppermute | solution.py:32
  175.8 3.3 %collective-permute-done.24.refs_4_ = bf16[256,512]{1,0:T(8,128)(2,1)S(1)} collective-permute-done((bf16[256,512]{1,0:T(8,128)(2,1)S(1)}, bf16[256,512]{1,0:T(8,128)(2,1)S(1)}, u32[]{:S(2)}, u32[]{:S(2)}) %collective-permute-start.24) | collective-permute-done | bytes 262176 | tf_op jit(solution)/shard_map/ppermute | solution.py:32
  179.2 1.4 collective-permute-done.23.refs_3_
  180.6 11.9 %shard_map.83 = (bf16[528,512]{1,0:T(8,128)(2,1)S(1)}, bf16[528,512]{1,0:T(8,128)(2,1)S(1)}, bf16[528,512]{1,0:T(8,128)(2,1)S(1)}, bf16[272,512]{1,0:T(8,128)(2,1)S(1)}, bf16[256,512]{1,0:T(8,128)(2,1)S(1)}) custom-call(bf16[528,512]{1,0:T(8,128)(2,1)S(1)} %add_convert_fusion.refs_0_, bf16[528,512]{1,0:T(8,128)(2,1)S(1)} %collective-permute-done.21.refs_1_, ...), custom_call_target="tpu_custom_call" | custom-call | flops 4429185024 | bytes 8388608 | tf_op jit(solution)/shard_map/pallas_call | solution.py:244
  192.5 2.2 %collective-permute-start.36 = (bf16[256,512]{1,0:T(8,128)(2,1)S(1)}, bf16[256,512]{1,0:T(8,128)(2,1)S(1)}, u32[]{:S(2)}, u32[]{:S(2)}) collective-permute-start(bf16[256,512]{1,0:T(8,128)(2,1)S(1)} %get-tuple-element.24), channel_id=1, source_target_pairs={{0,3},{1,0},{2,1},{3,2},{4,7},{5,4},{6,5},{7,6},{8,11},{9,8},{10,9... | collective-permute-start | bytes 786440 | tf_op jit(solution)/shard_map/ppermute | solution.py:32
  194.9 3.2 %collective-permute-done.36 = bf16[256,512]{1,0:T(8,128)(2,1)S(1)} collective-permute-done((bf16[256,512]{1,0:T(8,128)(2,1)S(1)}, bf16[256,512]{1,0:T(8,128)(2,1)S(1)}, u32[]{:S(2)}, u32[]{:S(2)}) %collective-permute-start.36) | collective-permute-done | bytes 262176 | tf_op jit(solution)/shard_map/ppermute | solution.py:32
  198.2 3.2 %collective-permute-start.37 = (bf16[528,512]{1,0:T(8,128)(2,1)S(1)}, bf16[528,512]{1,0:T(8,128)(2,1)S(1)}, u32[]{:S(2)}, u32[]{:S(2)}) collective-permute-start(bf16[528,512]{1,0:T(8,128)(2,1)S(1)} %pad_maximum_fusion.10), channel_id=1, source_target_pairs={{0,3},{1,0},{2,1},{3,2},{4,7},{5,4},{6,5},{7,6},{8,11},{9,8},{10,9... | collective-permute-start | bytes 1622024 | tf_op jit(solution)/shard_map/ppermute | solution.py:32
  201.7 7.2 %collective-permute-done.37 = bf16[528,512]{1,0:T(8,128)(2,1)S(1)} collective-permute-done((bf16[528,512]{1,0:T(8,128)(2,1)S(1)}, bf16[528,512]{1,0:T(8,128)(2,1)S(1)}, u32[]{:S(2)}, u32[]{:S(2)}) %collective-permute-start.37) | collective-permute-done | bytes 540704 | tf_op jit(solution)/shard_map/ppermute | solution.py:32
  208.9 3.4 %collective-permute-done.35 = bf16[528,512]{1,0:T(8,128)(2,1)S(1)} collective-permute-done((bf16[528,512]{1,0:T(8,128)(2,1)S(1)}, bf16[528,512]{1,0:T(8,128)(2,1)S(1)}, u32[]{:S(2)}, u32[]{:S(2)}) %collective-permute-start.35) | collective-permute-done | bytes 540704 | tf_op jit(solution)/shard_map/ppermute | solution.py:32
  212.3 1.1 add_convert_fusion.1
  (101 shorter events, 6.9 us)
Async XLA Ops:
  6.7 7.6 %collective-permute-start.11 = (bf16[2,64,512]{2,1,0:T(8,128)(2,1)S(1)}, bf16[2,64,512]{2,1,0:T(8,128)(2,1)S(1)}, u32[]{:S(2)}, u32[]{:S(2)}) collective-permute-start(bf16[2,64,512]{2,1,0:T(8,128)(2,1)S(1)} %get-tuple-element.32), channel_id=1, source_target_pairs={{0,64},{32,96},{64,128},{96,160},{128,192},{160,224},{192,0},{224,... | collective-permute-start | bytes 393224 | tf_op jit(solution)/shard_map/ppermute | solution.py:27
  11.0 5.0 %collective-permute-start.10 = (bf16[2,64,512]{2,1,0:T(8,128)(2,1)S(1)}, bf16[2,64,512]{2,1,0:T(8,128)(2,1)S(1)}, u32[]{:S(2)}, u32[]{:S(2)}) collective-permute-start(bf16[2,64,512]{2,1,0:T(8,128)(2,1)S(1)} %get-tuple-element.32), channel_id=1, source_target_pairs={{0,32},{32,64},{64,96},{96,128},{128,160},{160,192},{192,224},{224... | collective-permute-start | bytes 393224 | tf_op jit(solution)/shard_map/ppermute | solution.py:27
  16.0 6.8 %collective-permute-start.12 = (bf16[3,64,512]{2,1,0:T(8,128)(2,1)S(1)}, bf16[3,64,512]{2,1,0:T(8,128)(2,1)S(1)}, u32[]{:S(2)}, u32[]{:S(2)}) collective-permute-start(bf16[3,64,512]{2,1,0:T(8,128)(2,1)S(1)} %pad_maximum_fusion.15), channel_id=1, source_target_pairs={{0,64},{32,96},{64,128},{96,160},{128,192},{160,224},{192,0},{224,... | collective-permute-start | bytes 589832 | tf_op jit(solution)/shard_map/ppermute | solution.py:27
  22.9 7.3 %collective-permute-start.13 = (bf16[8,64,512]{2,1,0:T(8,128)(2,1)S(1)}, bf16[8,64,512]{2,1,0:T(8,128)(2,1)S(1)}, u32[]{:S(2)}, u32[]{:S(2)}) collective-permute-start(bf16[8,64,512]{2,1,0:T(8,128)(2,1)S(1)} %pad_maximum_fusion.11), channel_id=1, source_target_pairs={{0,4},{4,0},{1,5},{5,1},{2,6},{6,2},{3,7},{7,3},{8,12},{12,8},{9,1... | collective-permute-start | bytes 1572872 | tf_op jit(solution)/shard_map/ppermute | solution.py:20
  26.9 9.9 %collective-permute-start.25 = (bf16[4,64,512]{2,1,0:T(8,128)(2,1)S(1)}, bf16[4,64,512]{2,1,0:T(8,128)(2,1)S(1)}, u32[]{:S(2)}, u32[]{:S(2)}) collective-permute-start(bf16[4,64,512]{2,1,0:T(8,128)(2,1)S(1)} %get-tuple-element.28), channel_id=1, source_target_pairs={{0,8},{8,16},{16,24},{24,0},{4,28},{12,4},{20,12},{28,20},{1,9},{9... | collective-permute-start | bytes 786440 | tf_op jit(solution)/shard_map/ppermute | solution.py:27
  29.7 9.2 %copy-start.10 = (bf16[2,64,512]{2,1,0:T(8,128)(2,1)S(1)}, bf16[2,64,512]{2,1,0:T(8,128)(2,1)}, u32[]{:S(2)}) copy-start(bf16[2,64,512]{2,1,0:T(8,128)(2,1)} %get-tuple-element.31) | copy-start | bytes 393220
  29.7 7.1 %collective-permute-start.26 = (bf16[2,64,512]{2,1,0:T(8,128)(2,1)S(1)}, bf16[2,64,512]{2,1,0:T(8,128)(2,1)S(1)}, u32[]{:S(2)}, u32[]{:S(2)}) collective-permute-start(bf16[2,64,512]{2,1,0:T(8,128)(2,1)S(1)} %dynamic-slice_bitcast_fusion), channel_id=1, source_target_pairs={{0,16},{8,24},{16,0},{24,8},{4,20},{12,28},{20,4},{28,12},{1,17},{... | collective-permute-start | bytes 393224 | tf_op jit(solution)/shard_map/ppermute | solution.py:27
  30.3 25.3 %copy-start = (bf16[16,64,512]{2,1,0:T(8,128)(2,1)}, bf16[16,64,512]{2,1,0:T(8,128)(2,1)S(1)}, u32[]{:S(2)}) copy-start(bf16[16,64,512]{2,1,0:T(8,128)(2,1)S(1)} %pad_maximum_fusion.4.refs_12_) | copy-start | bytes 3145732
  30.3 26.6 %collective-permute-start.14 = (bf16[16,64,512]{2,1,0:T(8,128)(2,1)S(1)}, bf16[16,64,512]{2,1,0:T(8,128)(2,1)S(1)}, u32[]{:S(2)}, u32[]{:S(2)}) collective-permute-start(bf16[16,64,512]{2,1,0:T(8,128)(2,1)S(1)} %pad_maximum_fusion.4.refs_12_), channel_id=1, source_target_pairs={{0,8},{8,16},{16,24},{24,0},{4,28},{12,4},{20,12},{28,20},{1,9},{9... | collective-permute-start | bytes 3145736 | tf_op jit(solution)/shard_map/ppermute | solution.py:27
  36.9 18.6 %collective-permute-start.27 = (bf16[8,64,512]{2,1,0:T(8,128)(2,1)S(1)}, bf16[8,64,512]{2,1,0:T(8,128)(2,1)S(1)}, u32[]{:S(2)}, u32[]{:S(2)}) collective-permute-start(bf16[8,64,512]{2,1,0:T(8,128)(2,1)S(1)} %pad_maximum_fusion.12), channel_id=1, source_target_pairs={{0,4},{4,0},{1,5},{5,1},{2,6},{6,2},{3,7},{7,3},{8,12},{12,8},{9,1... | collective-permute-start | bytes 1572872 | tf_op jit(solution)/shard_map/ppermute | solution.py:20
  38.9 11.0 %collective-permute-start.1 = (bf16[2,64,512]{2,1,0:T(8,128)(2,1)S(1)}, bf16[2,64,512]{2,1,0:T(8,128)(2,1)S(1)}, u32[]{:S(2)}, u32[]{:S(2)}) collective-permute-start(bf16[2,64,512]{2,1,0:T(8,128)(2,1)S(1)} %copy-done.10), channel_id=1, source_target_pairs={{0,8},{8,16},{16,24},{24,0},{4,28},{12,4},{20,12},{28,20},{1,9},{9... | collective-permute-start | bytes 393224 | tf_op jit(solution)/shard_map/ppermute | solution.py:27
  39.2 5.3 %collective-permute-start.2 = (bf16[1,64,512]{2,1,0:T(8,128)(2,1)S(1)}, bf16[1,64,512]{2,1,0:T(8,128)(2,1)S(1)}, u32[]{:S(2)}, u32[]{:S(2)}) collective-permute-start(bf16[1,64,512]{2,1,0:T(8,128)(2,1)S(1)} %dynamic-slice_bitcast_fusion.2), channel_id=1, source_target_pairs={{0,16},{8,24},{16,0},{24,8},{4,20},{12,28},{20,4},{28,12},{1,17},{... | collective-permute-start | bytes 196616 | tf_op jit(solution)/shard_map/ppermute | solution.py:27
  49.9 7.0 %copy-start.13 = (s32[512]{0:T(512)S(1)}, s32[512]{0:T(512)}, u32[]{:S(2)}) copy-start(s32[512]{0:T(512)} %param.9) | copy-start | bytes 6148
  54.7 8.6 %collective-permute-start.3 = (bf16[8,64,512]{2,1,0:T(8,128)(2,1)}, bf16[8,64,512]{2,1,0:T(8,128)(2,1)}, u32[]{:S(2)}, u32[]{:S(2)}) collective-permute-start(bf16[8,64,512]{2,1,0:T(8,128)(2,1)} %all_gather.15.refs_4_), channel_id=1, source_target_pairs={{0,32},{32,64},{64,96},{96,128},{128,160},{160,192},{192,224},{224... | collective-permute-start | bytes 1572872 | tf_op jit(solution)/shard_map/ppermute | solution.py:27
  55.6 19.1 %collective-permute-start.28 = (bf16[16,64,512]{2,1,0:T(8,128)(2,1)S(1)}, bf16[16,64,512]{2,1,0:T(8,128)(2,1)}, u32[]{:S(2)}, u32[]{:S(2)}) collective-permute-start(bf16[16,64,512]{2,1,0:T(8,128)(2,1)S(1)} %pad_maximum_fusion.5.refs_8_), channel_id=1, source_target_pairs={{0,32},{32,64},{64,96},{96,128},{128,160},{160,192},{192,224},{224... | collective-permute-start | bytes 3145736 | tf_op jit(solution)/shard_map/ppermute | solution.py:27
  56.9 1.7 copy-start.6
  57.8 14.5 %collective-permute-start.15 = (bf16[8,64,512]{2,1,0:T(8,128)(2,1)}, bf16[8,64,512]{2,1,0:T(8,128)(2,1)S(1)}, u32[]{:S(2)}, u32[]{:S(2)}) collective-permute-start(bf16[8,64,512]{2,1,0:T(8,128)(2,1)} %slice.101), channel_id=1, source_target_pairs={{0,8},{8,16},{16,24},{24,0},{4,28},{12,4},{20,12},{28,20},{1,9},{9... | collective-permute-start | bytes 1572872 | tf_op jit(solution)/shard_map/ppermute | solution.py:27
  58.6 6.7 %collective-permute-start = (bf16[8,640]{1,0:T(8,128)(2,1)S(1)}, bf16[8,640]{1,0:T(8,128)(2,1)S(1)}, u32[]{:S(2)}, u32[]{:S(2)}) collective-permute-start(bf16[8,640]{1,0:T(8,128)(2,1)S(1)} %get-tuple-element.25), channel_id=1, source_target_pairs={{8,4},{16,12},{24,20},{32,28},{40,36},{48,44},{56,52},{64,60},{72,... | collective-permute-start | bytes 30728 | tf_op jit(solution)/shard_map/ppermute | solution.py:40
  63.4 17.0 %collective-permute-start.4 = (bf16[8,64,512]{2,1,0:T(8,128)(2,1)}, bf16[8,64,512]{2,1,0:T(8,128)(2,1)S(1)}, u32[]{:S(2)}, u32[]{:S(2)}) collective-permute-start(bf16[8,64,512]{2,1,0:T(8,128)(2,1)} %collective-permute-done.3.refs_5_), channel_id=1, source_target_pairs={{0,32},{32,64},{64,96},{96,128},{128,160},{160,192},{192,224},{224... | collective-permute-start | bytes 1572872 | tf_op jit(solution)/shard_map/ppermute | solution.py:27
  65.3 0.9 copy-start.8
  67.8 41.7 %all-to-all-start = ((bf16[4,528,512]{2,1,0:T(8,128)(2,1)}), bf16[4,528,512]{2,1,0:T(8,128)(2,1)}, u32[]{:S(2)}, u32[]{:S(2)}) async-start(bf16[4,528,512]{2,1,0:T(8,128)(2,1)} %broadcast_in_dim.14), calls=%async_computation | async-start | bytes 4325376 | tf_op jit(solution)/shard_map/all_to_all | solution.py:131
  72.3 1.3 copy-start.2
  73.6 27.2 %copy-start.11 = (f32[2,2048]{1,0:T(2,128)S(1)}, f32[2,2048]{1,0:T(2,128)}, u32[]{:S(2)}) copy-start(f32[2,2048]{1,0:T(2,128)} %param.10) | copy-start | bytes 49156
  73.6 27.2 %copy-start.12 = (f32[2,3,512]{2,0,1:T(2,128)S(1)}, f32[2,3,512]{2,0,1:T(2,128)}, u32[]{:S(2)}) copy-start(f32[2,3,512]{2,0,1:T(2,128)} %param.14) | copy-start | bytes 36868
  73.6 37.0 %collective-permute-start.16 = (bf16[24,64,512]{2,1,0:T(8,128)(2,1)}, bf16[24,64,512]{2,1,0:T(8,128)(2,1)}, u32[]{:S(2)}, u32[]{:S(2)}) collective-permute-start(bf16[24,64,512]{2,1,0:T(8,128)(2,1)} %pad_maximum_fusion.1), channel_id=1, source_target_pairs={{0,4},{4,0},{1,5},{5,1},{2,6},{6,2},{3,7},{7,3},{8,12},{12,8},{9,1... | collective-permute-start | bytes 4718600 | tf_op jit(solution)/shard_map/ppermute | solution.py:20
  74.1 26.7 %copy-start.7 = (bf16[512,512]{1,0:T(8,128)(2,1)S(1)}, bf16[512,512]{1,0:T(8,128)(2,1)}, u32[]{:S(2)}) copy-start(bf16[512,512]{1,0:T(8,128)(2,1)} %param.8) | copy-start | bytes 1572868
  74.7 34.4 %collective-permute-start.29 = (bf16[16,64,512]{2,1,0:T(8,128)(2,1)}, bf16[16,64,512]{2,1,0:T(8,128)(2,1)}, u32[]{:S(2)}, u32[]{:S(2)}) collective-permute-start(bf16[16,64,512]{2,1,0:T(8,128)(2,1)} %collective-permute-done.28.refs_9_), channel_id=1, source_target_pairs={{0,32},{32,64},{64,96},{96,128},{128,160},{160,192},{192,224},{224... | collective-permute-start | bytes 3145736 | tf_op jit(solution)/shard_map/ppermute | solution.py:27
  80.3 20.5 %copy-start.4 = (bf16[8,64,512]{2,1,0:T(8,128)(2,1)}, bf16[8,64,512]{2,1,0:T(8,128)(2,1)S(1)}, u32[]{:S(2)}) copy-start(bf16[8,64,512]{2,1,0:T(8,128)(2,1)S(1)} %collective-permute-done.4.refs_6_) | copy-start | bytes 1572868
  80.3 16.9 %collective-permute-start.5 = (bf16[8,64,512]{2,1,0:T(8,128)(2,1)S(1)}, bf16[8,64,512]{2,1,0:T(8,128)(2,1)}, u32[]{:S(2)}, u32[]{:S(2)}) collective-permute-start(bf16[8,64,512]{2,1,0:T(8,128)(2,1)S(1)} %collective-permute-done.4.refs_6_), channel_id=1, source_target_pairs={{0,32},{32,64},{64,96},{96,128},{128,160},{160,192},{192,224},{224... | collective-permute-start | bytes 1572872 | tf_op jit(solution)/shard_map/ppermute | solution.py:27
  84.4 25.0 %collective-permute-start.7 = (bf16[16,64,512]{2,1,0:T(8,128)(2,1)}, bf16[16,64,512]{2,1,0:T(8,128)(2,1)}, u32[]{:S(2)}, u32[]{:S(2)}) collective-permute-start(bf16[16,64,512]{2,1,0:T(8,128)(2,1)} %pad_maximum_fusion.3), channel_id=1, source_target_pairs={{0,4},{4,0},{1,5},{5,1},{2,6},{6,2},{3,7},{7,3},{8,12},{12,8},{9,1... | collective-permute-start | bytes 3145736 | tf_op jit(solution)/shard_map/ppermute | solution.py:20
  98.8 5.5 %collective-permute-start.6 = (bf16[4,64,512]{2,1,0:T(8,128)(2,1)}, bf16[4,64,512]{2,1,0:T(8,128)(2,1)}, u32[]{:S(2)}, u32[]{:S(2)}) collective-permute-start(bf16[4,64,512]{2,1,0:T(8,128)(2,1)} %constant_dynamic-slice_fusion.1), channel_id=1, source_target_pairs={{0,32},{32,64},{64,96},{96,128},{128,160},{160,192},{192,224},{224... | collective-permute-start | bytes 786440 | tf_op jit(solution)/shard_map/ppermute | solution.py:27
  101.0 9.6 %collective-permute-start.8 = (bf16[8,64,512]{2,1,0:T(8,128)(2,1)}, bf16[8,64,512]{2,1,0:T(8,128)(2,1)}, u32[]{:S(2)}, u32[]{:S(2)}) collective-permute-start(bf16[8,64,512]{2,1,0:T(8,128)(2,1)} %collective-permute-done.5.refs_7_), channel_id=1, source_target_pairs={{0,4},{4,0},{1,5},{5,1},{2,6},{6,2},{3,7},{7,3},{8,12},{12,8},{9,1... | collective-permute-start | bytes 1572872 | tf_op jit(solution)/shard_map/ppermute | solution.py:20
  104.4 6.2 %collective-permute-start.9 = (bf16[4,64,512]{2,1,0:T(8,128)(2,1)}, bf16[4,64,512]{2,1,0:T(8,128)(2,1)}, u32[]{:S(2)}, u32[]{:S(2)}) collective-permute-start(bf16[4,64,512]{2,1,0:T(8,128)(2,1)} %collective-permute-done.6.refs_8_), channel_id=1, source_target_pairs={{0,4},{4,0},{1,5},{5,1},{2,6},{6,2},{3,7},{7,3},{8,12},{12,8},{9,1... | collective-permute-start | bytes 786440 | tf_op jit(solution)/shard_map/ppermute | solution.py:20
  109.1 23.4 %collective-permute-start.30 = (bf16[16,64,512]{2,1,0:T(8,128)(2,1)}, bf16[16,64,512]{2,1,0:T(8,128)(2,1)S(1)}, u32[]{:S(2)}, u32[]{:S(2)}) collective-permute-start(bf16[16,64,512]{2,1,0:T(8,128)(2,1)} %collective-permute-done.29.refs_10_), channel_id=1, source_target_pairs={{0,32},{32,64},{64,96},{96,128},{128,160},{160,192},{192,224},{224... | collective-permute-start | bytes 3145736 | tf_op jit(solution)/shard_map/ppermute | solution.py:27
  110.6 1.2 copy-start.1
  111.8 1.0 copy-start.3
  112.8 1.0 copy-start.5
  127.5 7.8 %collective-permute-start.19 = (bf16[256,512]{1,0:T(8,128)(2,1)S(1)}, bf16[256,512]{1,0:T(8,128)(2,1)S(1)}, u32[]{:S(2)}, u32[]{:S(2)}) collective-permute-start(bf16[256,512]{1,0:T(8,128)(2,1)S(1)} %get-tuple-element.19), channel_id=1, source_target_pairs={{0,3},{1,0},{2,1},{3,2},{4,7},{5,4},{6,5},{7,6},{8,11},{9,8},{10,9... | collective-permute-start | bytes 786440 | tf_op jit(solution)/shard_map/ppermute | solution.py:32
  131.7 44.1 %collective-permute-start.32 = (bf16[32,64,512]{2,1,0:T(8,128)(2,1)S(1)}, bf16[32,64,512]{2,1,0:T(8,128)(2,1)S(1)}, u32[]{:S(2)}, u32[]{:S(2)}) collective-permute-start(bf16[32,64,512]{2,1,0:T(8,128)(2,1)S(1)} %pad_maximum_fusion), channel_id=1, source_target_pairs={{0,4},{4,0},{1,5},{5,1},{2,6},{6,2},{3,7},{7,3},{8,12},{12,8},{9,1... | collective-permute-start | bytes 6291464 | tf_op jit(solution)/shard_map/ppermute | solution.py:20
  132.5 11.2 %collective-permute-start.31 = (bf16[8,64,512]{2,1,0:T(8,128)(2,1)S(1)}, bf16[8,64,512]{2,1,0:T(8,128)(2,1)S(1)}, u32[]{:S(2)}, u32[]{:S(2)}) collective-permute-start(bf16[8,64,512]{2,1,0:T(8,128)(2,1)S(1)} %slice.105), channel_id=1, source_target_pairs={{0,32},{32,64},{64,96},{96,128},{128,160},{160,192},{192,224},{224... | collective-permute-start | bytes 1572872 | tf_op jit(solution)/shard_map/ppermute | solution.py:27
  134.1 9.1 %collective-permute-start.17 = (bf16[272,512]{1,0:T(8,128)(2,1)S(1)}, bf16[272,512]{1,0:T(8,128)(2,1)S(1)}, u32[]{:S(2)}, u32[]{:S(2)}) collective-permute-start(bf16[272,512]{1,0:T(8,128)(2,1)S(1)} %get-tuple-element.17), channel_id=1, source_target_pairs={{0,1},{1,2},{2,3},{3,0},{4,5},{5,6},{6,7},{7,4},{8,9},{9,10},{10,1... | collective-permute-start | bytes 835592 | tf_op jit(solution)/shard_map/ppermute | solution.py:32
  135.4 13.9 %collective-permute-start.20 = (bf16[528,512]{1,0:T(8,128)(2,1)S(1)}, bf16[528,512]{1,0:T(8,128)(2,1)S(1)}, u32[]{:S(2)}, u32[]{:S(2)}) collective-permute-start(bf16[528,512]{1,0:T(8,128)(2,1)S(1)} %pad_maximum_fusion.8), channel_id=1, source_target_pairs={{0,3},{1,0},{2,1},{3,2},{4,7},{5,4},{6,5},{7,6},{8,11},{9,8},{10,9... | collective-permute-start | bytes 1622024 | tf_op jit(solution)/shard_map/ppermute | solution.py:32
  143.4 15.2 %copy-start.9 = (bf16[528,640]{1,0:T(8,128)(2,1)S(1)}, bf16[528,640]{1,0:T(8,128)(2,1)}, u32[]{:S(2)}) copy-start(bf16[528,640]{1,0:T(8,128)(2,1)} %copy-done.8) | copy-start | bytes 2027524
  143.4 15.2 %collective-permute-start.18 = (bf16[528,512]{1,0:T(8,128)(2,1)S(1)}, bf16[528,512]{1,0:T(8,128)(2,1)S(1)}, u32[]{:S(2)}, u32[]{:S(2)}) collective-permute-start(bf16[528,512]{1,0:T(8,128)(2,1)S(1)} %pad_maximum_fusion.7), channel_id=1, source_target_pairs={{0,1},{1,2},{2,3},{3,0},{4,5},{5,6},{6,7},{7,4},{8,9},{9,10},{10,1... | collective-permute-start | bytes 1622024 | tf_op jit(solution)/shard_map/ppermute | solution.py:32
  143.9 36.7 %collective-permute-start.33 = (bf16[24,64,512]{2,1,0:T(8,128)(2,1)S(1)}, bf16[24,64,512]{2,1,0:T(8,128)(2,1)S(1)}, u32[]{:S(2)}, u32[]{:S(2)}) collective-permute-start(bf16[24,64,512]{2,1,0:T(8,128)(2,1)S(1)} %pad_maximum_fusion.2), channel_id=1, source_target_pairs={{0,4},{4,0},{1,5},{5,1},{2,6},{6,2},{3,7},{7,3},{8,12},{12,8},{9,1... | collective-permute-start | bytes 4718600 | tf_op jit(solution)/shard_map/ppermute | solution.py:20
  158.9 14.1 %collective-permute-start.21 = (bf16[528,512]{1,0:T(8,128)(2,1)S(1)}, bf16[528,512]{1,0:T(8,128)(2,1)S(1)}, u32[]{:S(2)}, u32[]{:S(2)}) collective-permute-start(bf16[528,512]{1,0:T(8,128)(2,1)S(1)} %add_convert_fusion.refs_0_), channel_id=1, source_target_pairs={{0,1},{1,2},{2,3},{3,0},{4,5},{5,6},{6,7},{7,4},{8,9},{9,10},{10,1... | collective-permute-start | bytes 1622024 | tf_op jit(solution)/shard_map/ppermute | solution.py:32
  158.9 14.1 %collective-permute-start.22 = (bf16[528,512]{1,0:T(8,128)(2,1)S(1)}, bf16[528,512]{1,0:T(8,128)(2,1)S(1)}, u32[]{:S(2)}, u32[]{:S(2)}) collective-permute-start(bf16[528,512]{1,0:T(8,128)(2,1)S(1)} %add_convert_fusion.refs_0_), channel_id=1, source_target_pairs={{0,3},{1,0},{2,1},{3,2},{4,7},{5,4},{6,5},{7,6},{8,11},{9,8},{10,9... | collective-permute-start | bytes 1622024 | tf_op jit(solution)/shard_map/ppermute | solution.py:32
  173.0 7.6 %collective-permute-start.23 = (bf16[272,512]{1,0:T(8,128)(2,1)S(1)}, bf16[272,512]{1,0:T(8,128)(2,1)S(1)}, u32[]{:S(2)}, u32[]{:S(2)}) collective-permute-start(bf16[272,512]{1,0:T(8,128)(2,1)S(1)} %slice.102), channel_id=1, source_target_pairs={{0,1},{1,2},{2,3},{3,0},{4,5},{5,6},{6,7},{7,4},{8,9},{9,10},{10,1... | collective-permute-start | bytes 835592 | tf_op jit(solution)/shard_map/ppermute | solution.py:32
  173.1 6.1 %collective-permute-start.24 = (bf16[256,512]{1,0:T(8,128)(2,1)S(1)}, bf16[256,512]{1,0:T(8,128)(2,1)S(1)}, u32[]{:S(2)}, u32[]{:S(2)}) collective-permute-start(bf16[256,512]{1,0:T(8,128)(2,1)S(1)} %slice.103), channel_id=1, source_target_pairs={{0,3},{1,0},{2,1},{3,2},{4,7},{5,4},{6,5},{7,6},{8,11},{9,8},{10,9... | collective-permute-start | bytes 786440 | tf_op jit(solution)/shard_map/ppermute | solution.py:32
  192.5 5.5 %collective-permute-start.36 = (bf16[256,512]{1,0:T(8,128)(2,1)S(1)}, bf16[256,512]{1,0:T(8,128)(2,1)S(1)}, u32[]{:S(2)}, u32[]{:S(2)}) collective-permute-start(bf16[256,512]{1,0:T(8,128)(2,1)S(1)} %get-tuple-element.24), channel_id=1, source_target_pairs={{0,3},{1,0},{2,1},{3,2},{4,7},{5,4},{6,5},{7,6},{8,11},{9,8},{10,9... | collective-permute-start | bytes 786440 | tf_op jit(solution)/shard_map/ppermute | solution.py:32
  194.8 6.7 %collective-permute-start.34 = (bf16[272,512]{1,0:T(8,128)(2,1)S(1)}, bf16[272,512]{1,0:T(8,128)(2,1)S(1)}, u32[]{:S(2)}, u32[]{:S(2)}) collective-permute-start(bf16[272,512]{1,0:T(8,128)(2,1)S(1)} %get-tuple-element.22), channel_id=1, source_target_pairs={{0,1},{1,2},{2,3},{3,0},{4,5},{5,6},{6,7},{7,4},{8,9},{9,10},{10,1... | collective-permute-start | bytes 835592 | tf_op jit(solution)/shard_map/ppermute | solution.py:32
  198.2 10.7 %collective-permute-start.37 = (bf16[528,512]{1,0:T(8,128)(2,1)S(1)}, bf16[528,512]{1,0:T(8,128)(2,1)S(1)}, u32[]{:S(2)}, u32[]{:S(2)}) collective-permute-start(bf16[528,512]{1,0:T(8,128)(2,1)S(1)} %pad_maximum_fusion.10), channel_id=1, source_target_pairs={{0,3},{1,0},{2,1},{3,2},{4,7},{5,4},{6,5},{7,6},{8,11},{9,8},{10,9... | collective-permute-start | bytes 1622024 | tf_op jit(solution)/shard_map/ppermute | solution.py:32
  201.6 10.7 %collective-permute-start.35 = (bf16[528,512]{1,0:T(8,128)(2,1)S(1)}, bf16[528,512]{1,0:T(8,128)(2,1)S(1)}, u32[]{:S(2)}, u32[]{:S(2)}) collective-permute-start(bf16[528,512]{1,0:T(8,128)(2,1)S(1)} %pad_maximum_fusion.9), channel_id=1, source_target_pairs={{0,1},{1,2},{2,3},{3,0},{4,5},{5,6},{6,7},{7,4},{8,9},{9,10},{10,1... | collective-permute-start | bytes 1622024 | tf_op jit(solution)/shard_map/ppermute | solution.py:32
